TPU v7x, 32 devices: a whole 2x2x4 slice. The times are simulated.
32 devices in a mesh: sp: 8 (over z, y), tp: 4 (over x, core).
Axes of the slice: x: 2, y: 2, z: 4, core: 2. Of those that a mesh axis runs over, the one named last changes fastest.
Arguments:
- query_one: bfloat16 [2048, 512], P('sp', 'tp'), may hold values from -190 to 190
- query_two: bfloat16 [2048, 512], P('sp', 'tp'), may hold values from -190 to 190
- key_one: bfloat16 [2048, 512], P('sp', 'tp'), may hold values from -10 to 10
- key_two: bfloat16 [2048, 512], P('sp', 'tp'), may hold values from -10 to 10
- values: bfloat16 [2048, 1024], P('sp', 'tp'), may hold values from -6 to 6
- mix_lambda: float32 [8], P('tp'), may hold values from 0.3 to 0.8
- head_gain: float32 [128], replicated, may hold values from 0.1 to 1.9
- stream: bfloat16 [2048, 2048], P('sp', 'tp'), may hold values from -6 to 6
- out_weight: bfloat16 [1024, 2048], P('tp'), may hold values from -0.1875 to 0.1875
- first_gain: float32 [2048], replicated, may hold values from 0.1 to 1.9
- up_weight: bfloat16 [2048, 4096], P('sp', 'tp'), may hold values from -0.125 to 0.125
- down_weight: bfloat16 [4096, 2048], P('tp', 'sp'), may hold values from -0.09375 to 0.09375
- second_gain: float32 [2048], replicated, may hold values from 0.1 to 1.9
Outputs:
- layer_out: bfloat16 [2048, 2048], P(('sp', 'tp'))
All inputs are finite; a program needn't handle non-finite values.
Results may differ from a plain program's by a relative error of at most 0.019.
Values may be sent and summed in bfloat16 or wider, within the bound.
A program may use at most 128 MiB of HBM per device.

v0:
```python
import functools
import math

import jax
import jax.numpy as jnp
from jax import lax
from jax.experimental import pallas as pl
from jax.experimental.pallas import tpu as pltpu
from jax.sharding import PartitionSpec as P

MESH = pl.DeviceIdType.MESH
F32, BF16 = jnp.float32, jnp.bfloat16
ALPHA = 2.0**0.5
NT = (((1,), (1,)), ((), ()))
TN = (((0,), (0,)), ((), ()))


def layer_norm(value, gain):
    centre = jnp.mean(value, axis=-1, keepdims=True)
    spread = jnp.mean(jnp.square(value - centre), axis=-1, keepdims=True)
    return (value - centre) * lax.rsqrt(spread + 1e-05) * gain


def kernel(
    nsp, ntp, heads,
    lam_ref, qkv_ref, hg_ref, st_ref, ow_ref, g1_ref, up_ref, dn_ref, g2_ref,
    out_ref,
    lam_all, q_buf, qm, m_run, l_run, acc, kv_buf, up_buf, dn_buf, ow_buf, st_buf, at_snd, at_buf,
    pre, h_own, h_buf, act, sib_snd, sib_buf, part, red_snd, red_buf,
    loc_sem, lms, qs, kvz, kvy, kvs, upz, upy, dnz, dny, owx, ows, sts, ats, hps, hss, sbs, rds,
):
    s, t = lax.axis_index("sp"), lax.axis_index("tp")
    nz, nth = nsp // 2, ntp // 2
    ng = 2 * nth
    z, y = s // 2, s % 2
    zh, zl = z // 2, z % 2
    th, tl = t // 2, t % 2
    sib_t = th * 2 + (1 - tl)
    y_sp = z * 2 + (1 - y)
    grp = zl * nth + th
    tok = qkv_ref.shape[1]
    share = tok // ntp
    fh = up_ref.shape[1] // 2
    vd = acc.shape[1]
    qw = q_buf.shape[2]
    qk = qw // 2
    tall = q_buf.shape[1]
    nzb = q_buf.shape[0]
    d = pre.shape[1]
    zq = lax.rem(z, nzb)
    zb = z - zq
    entry_t, head_j = zq // heads, lax.rem(zq, heads)
    entry = tl == entry_t
    head = th * nzb + zq

    def rc(src, dst, sems, i, sp, tp, arrive=None):
        arrive = i if arrive is None else arrive
        return pltpu.make_async_remote_copy(
            src_ref=src, dst_ref=dst, send_sem=sems.at[0, i], recv_sem=sems.at[1, arrive],
            device_id={"sp": sp, "tp": tp}, device_id_type=MESH,
        )

    def each(lo, hi, body):
        if hi - lo <= 4:
            for k in range(lo, hi):
                body(k)
        else:
            lax.fori_loop(lo, hi, lambda k, c: (body(k), c)[1], 0)

    def zto(k):
        return lax.rem(z + k, nz)

    def zfrom(k):
        return lax.rem(z + nz - k, nz)

    def slab(j):
        return qkv_ref.at[j, :, pl.ds(qw, qw + vd)]

    def q_c(j, hf):
        zd = zb + heads * tl + j
        return rc(
            qkv_ref.at[j, pl.ds(hf * tall, tall), pl.ds(0, qw)], q_buf.at[zq],
            qs, j * 2 + hf, zd * 2 + y, th * 2 + hf, zq,
        )

    def q_in(i):
        return rc(q_buf.at[i], q_buf.at[i], qs, 0, y_sp, t, i)

    def kv_z(j, r):
        zd = r * nzb + heads * tl + j
        return rc(
            slab(j), kv_buf.at[s], kvz, r * heads + j, zd * 2 + y, t, lax.rem(zd - z + nz, nz)
        )

    def kv_zin(k):
        b = zfrom(k) * 2 + y
        return rc(kv_buf.at[b], kv_buf.at[b], kvz, 0, y_sp, t, k)

    def kv_y(k):
        b = zfrom(k) * 2 + y
        return rc(kv_buf.at[b], kv_buf.at[b], kvy, k, y_sp, t)

    def kv_y0():
        return rc(slab(head_j), kv_buf.at[s], kvy, 0, y_sp, t)

    def kv_s(k, side):
        b = zfrom(k) * 2 + lax.rem(y + side, 2)
        return rc(kv_buf.at[b], kv_buf.at[b], kvs, side * nz + k, s, sib_t)

    def kv_s0():
        return rc(slab(head_j), kv_buf.at[s], kvs, 0, s, sib_t)

    def up_half(j):
        return up_ref.at[:, pl.ds(pl.multiple_of(j * fh, fh), fh)]

    def dn_half(j):
        return dn_ref.at[pl.ds(pl.multiple_of(j * fh, fh), fh), :]

    def up_z(k):
        zd = zto(k)
        return rc(up_half(zd % 2), up_buf.at[s], upz, k, zd * 2 + y, t)

    def dn_z(k):
        zd = zto(k)
        return rc(dn_half(zd % 2), dn_buf.at[s], dnz, k, zd * 2 + y, t)

    def up_y0():
        return rc(up_half(zl), up_buf.at[s], upy, 0, y_sp, t)

    def dn_y0():
        return rc(dn_half(zl), dn_buf.at[s], dny, 0, y_sp, t)

    def up_y(k):
        b = zfrom(k) * 2 + y
        return rc(up_buf.at[b], up_buf.at[b], upy, k, y_sp, t)

    def dn_y(k):
        b = zfrom(k) * 2 + y
        return rc(dn_buf.at[b], dn_buf.at[b], dny, k, y_sp, t)

    def ow_x(k):
        return rc(ow_ref, ow_buf.at[t], owx, k, s, lax.rem(th + k, nth) * 2 + tl)

    def ow_s0():
        return rc(ow_ref, ow_buf.at[t], ows, 0, s, sib_t)

    def ow_s(k):
        b = lax.rem(th + nth - k, nth) * 2 + tl
        return rc(ow_buf.at[b], ow_buf.at[b], ows, k, s, sib_t)

    def rows_of(tt):
        return pl.ds(pl.multiple_of(tt * share, share), share)

    def st_c(k):
        td = lax.rem(t + k, ntp)
        return rc(st_ref.at[rows_of(td), :], st_buf.at[t], sts, k, s, td)

    def at_c(i, u):
        rows = pl.ds(i * tall + u * share, share)
        cols = pl.ds(pl.multiple_of(head * vd, vd), vd)
        return rc(
            at_snd.at[rows, :], at_buf.at[:, cols], ats, i * nth + u,
            (zb + i) * 2 + y, tl * nth + u, head,
        )

    def at_in(hd):
        ref = at_buf.at[:, pl.ds(hd * vd, vd)]
        return rc(ref, ref, ats, 0, y_sp, t, hd)

    mine = t // nth == tl

    def at_self(hd):
        return mine & (head == hd)

    def grp_dev(g):
        return (zh * 2 + g // nth) * 2 + y, lax.rem(g, nth) * 2 + tl

    def h_p(k):
        sp, tp = grp_dev(lax.rem(grp + k, ng))
        return rc(h_own, h_buf.at[tl, grp], hps, k, sp, tp)

    def h_s0():
        return rc(h_own, h_buf.at[tl, grp], hss, 0, s, sib_t)

    def h_s(k):
        g = lax.rem(grp + ng - k, ng)
        return rc(h_buf.at[tl, g], h_buf.at[tl, g], hss, k, s, sib_t)

    def sib_c():
        return rc(sib_snd, sib_buf, sbs, 0, s, sib_t)

    def red_c(k):
        g = lax.rem(grp + k, ng)
        sp, tp = grp_dev(g)
        return rc(red_snd.at[g], red_buf.at[grp], rds, k, sp, tp)

    barrier = pltpu.get_barrier_semaphore()

    def greet(sp, tp):
        pl.semaphore_signal(barrier, inc=1, device_id={"sp": sp, "tp": tp}, device_id_type=MESH)

    for i in range(nzb):
        for tt in range(ntp):
            pl.when((i != zq) | (tt != t))(functools.partial(greet, (zb + i) * 2 + y, tt))
    if nz > nzb:
        each(0, nz, lambda k: pl.when((k < zb) | (k >= zb + nzb))(lambda: greet(k * 2 + y, t)))
    greet(y_sp, t)
    pl.semaphore_wait(barrier, nzb * ntp - 1 + nz - nzb + 1)

    def q_self(j, hf):
        return (zq == heads * tl + j) & (hf == tl)

    pairs = [(j, hf) for j in range(heads) for hf in range(2)]
    for j, hf in pairs:
        pl.when(jnp.logical_not(q_self(j, hf)))(lambda: q_c(j, hf).start())

        @pl.when(q_self(j, hf))
        def _():
            q_buf[zq] = qkv_ref[j, hf * tall : (hf + 1) * tall, :qw]

    def lam_c():
        return rc(lam_ref, lam_all.at[tl], lms, 0, s, sib_t)

    lam_all[tl] = lam_ref[...]

    def kv_out(fn):
        for j in range(heads):
            each(0, nz // nzb, lambda r: pl.when(r * nzb + heads * tl + j != z)(lambda: fn(kv_z(j, r))))

    kv_out(lambda c: c.start())

    @pl.when(entry)
    def _():
        kv_y0().start()
        kv_s0().start()
        kv_buf[s] = qkv_ref[head_j, :, qw:]

    lam_c().start()
    each(1, ntp, lambda k: st_c(k).start())
    each(1, nth, lambda k: ow_x(k).start())
    ow_s0().start()
    locals_ = [
        pltpu.make_async_copy(ow_ref, ow_buf.at[t], loc_sem.at[0]),
        pltpu.make_async_copy(up_half(zl), up_buf.at[s], loc_sem.at[1]),
        pltpu.make_async_copy(dn_half(zl), dn_buf.at[s], loc_sem.at[2]),
    ]
    for c in locals_:
        c.start()
    each(1, nz, lambda k: up_z(k).start())

    scale = qk ** (-0.5)
    m_run[...] = jnp.full(m_run.shape, -1e30, F32)
    l_run[...] = jnp.zeros(l_run.shape, F32)
    acc[...] = jnp.zeros(acc.shape, F32)
    lane = lax.broadcasted_iota(jnp.int32, (tall, qw), 1)
    for i in range(nzb):
        pl.when(jnp.logical_not((zq == i) & entry))(lambda: q_in(i).wait_recv())
        qv = q_buf[i].astype(F32) * scale
        for mp in range(2):
            keep = (lane >= mp * qk) & (lane < (mp + 1) * qk)
            qm[mp, i * tall : (i + 1) * tall, :] = jnp.where(keep, qv, 0.0).astype(BF16)

    def absorb(block):
        v = block[:, qw:]
        for r in range(2):
            sc = lax.dot_general(block[:, :qw], qm[r], NT, preferred_element_type=F32)
            old = m_run[r]
            new = jnp.maximum(old, jnp.max(sc, axis=0, keepdims=True))
            fac = jnp.exp(old - new)
            ex = jnp.exp(sc - new)
            l_run[r] = l_run[r] * fac + jnp.sum(ex, axis=0, keepdims=True)
            acc[r] = acc[r] * fac + lax.dot_general(
                v, ex.astype(BF16), TN, preferred_element_type=F32
            )
            m_run[r] = new

    def own_step():
        pl.when(jnp.logical_not(entry))(lambda: kv_s0().wait_recv())
        absorb(kv_buf.at[s])

    own_step()

    def z_step(k, c):
        @pl.when(entry)
        def _():
            kv_zin(k).wait_recv()
            kv_y(k).start()
            kv_s(k, 0).start()

        pl.when(jnp.logical_not(entry))(lambda: kv_s(k, 0).wait_recv())
        absorb(kv_buf.at[zfrom(k) * 2 + y])
        return c

    lax.fori_loop(1, nz, z_step, 0)
    up_y0().start()
    dn_y0().start()

    def y_step(k, c):
        @pl.when(entry)
        def _():
            kv_y(k).wait_recv()
            kv_s(k, 1).start()

        pl.when(jnp.logical_not(entry))(lambda: kv_s(k, 1).wait_recv())
        absorb(kv_buf.at[zfrom(k) * 2 + 1 - y])
        return c

    lax.fori_loop(0, nz, y_step, 0)
    up_z(1).wait_recv()
    up_y(1).start()

    for k in range(1, nth):
        ow_x(k).wait_recv()
        ow_s(k).start()

    lam_c().wait_recv()
    lam = lam_all[entry_t, head_j][:, :1]
    mixed = acc[0] / l_run[0] - lam * (acc[1] / l_run[1])
    inv = lax.rsqrt(jnp.mean(jnp.square(mixed), axis=0, keepdims=True) + 1e-05)
    normed = jnp.transpose(mixed * inv) * hg_ref[...] * 0.8
    at_snd[...] = normed.astype(BF16)
    spots = [(i, u) for i in range(nzb) for u in range(nth)]
    for i, u in spots:
        own = (zq == i) & (tl * nth + u == t)
        pl.when(jnp.logical_not(own))(lambda: at_c(i, u).start())

        @pl.when(own)
        def _():
            cols = pl.ds(pl.multiple_of(head * vd, vd), vd)
            at_buf[:, cols] = at_snd[i * tall + u * share : i * tall + (u + 1) * share, :]

    st_buf[t] = st_ref[rows_of(t), :]
    up_z(2).wait_recv()
    up_y(2).start()

    each(1, ntp, lambda k: st_c(k).wait_recv())
    cols = st_ref.shape[1]
    for b in range(ntp):
        pre[:, b * cols : (b + 1) * cols] = ALPHA * st_buf[b].astype(F32)
    locals_[0].wait()
    ow_s0().wait_recv()
    for k in range(1, nth):
        ow_s(k).wait_recv()
    for hd in range(nzb * nth):
        pl.when(jnp.logical_not(at_self(hd)))(lambda: at_in(hd).wait_recv())
    for b in range(ntp):
        at = slice(b * cols, (b + 1) * cols)
        full = ow_buf[:, :, at].reshape(at_buf.shape[1], cols)
        pre[:, at] += jnp.dot(at_buf[...], full, preferred_element_type=F32)
    h_own[...] = layer_norm(pre[...], g1_ref[...]).astype(BF16)
    each(1, ng, lambda k: h_p(k).start())
    h_s0().start()
    each(1, nz, lambda k: dn_z(k).start())
    h_buf[tl, grp] = h_own[...]

    def up_fwd(k):
        up_z(k).wait_recv()
        up_y(k).start()

    each(3, nz, up_fwd)

    def h_fwd(k):
        h_p(k).wait_recv()
        h_s(k).start()

    def dn_fwd(k):
        dn_z(k).wait_recv()
        dn_y(k).start()

    each(1, ng, h_fwd)
    dn_fwd(1)
    h_s0().wait_recv()
    each(1, ng, lambda k: h_s(k).wait_recv())
    locals_[1].wait()
    up_y0().wait_recv()
    each(1, nz, lambda k: up_y(k).wait_recv())

    half = ng * share
    depth = up_buf.shape[1]
    for side in range(2):
        for c in range(2 if fh % 256 == 0 else 1):
            wide = fh // (2 if fh % 256 == 0 else 1)
            at = slice(c * wide, (c + 1) * wide)
            hid = h_buf[side].reshape(half, d)
            w = up_buf[:, :, at].reshape(d, wide)
            up = jnp.dot(hid, w, preferred_element_type=F32)
            act[side, :, at] = jnp.square(jnp.maximum(up, 0.0)).astype(BF16)

    each(2, nz, dn_fwd)
    locals_[2].wait()
    dn_y0().wait_recv()
    each(1, nz, lambda k: dn_y(k).wait_recv())
    out_w = dn_buf.shape[2]
    for b in range(nsp):
        at = slice(b * out_w, (b + 1) * out_w)
        res = jnp.dot(act[1 - tl], dn_buf[b], preferred_element_type=F32)
        sib_snd[:, at] = res.astype(BF16)
    sib_c().start()
    for b in range(nsp):
        at = slice(b * out_w, (b + 1) * out_w)
        part[:, at] = jnp.dot(act[tl], dn_buf[b], preferred_element_type=F32)
    sib_c().wait_recv()

    def red_step(k):
        g = lax.rem(grp + k, ng)
        rows = pl.ds(pl.multiple_of(g * share, share), share)
        red_snd[g] = (part[rows, :] + sib_buf[rows, :].astype(F32)).astype(BF16)
        red_c(k).start()

    for k in range(ng - 1, 0, -1):
        red_step(k)
    rows = pl.ds(pl.multiple_of(grp * share, share), share)
    pre[...] = part[rows, :] + sib_buf[rows, :].astype(F32) + ALPHA * h_own[...].astype(F32)
    for k in range(ng - 1, 0, -1):
        red_c(k).wait_recv()
        pre[...] += red_buf[lax.rem(grp + ng - k, ng)].astype(F32)
    out_ref[...] = layer_norm(pre[...], g2_ref[...]).astype(BF16)

    for j, hf in pairs:
        pl.when(jnp.logical_not(q_self(j, hf)))(lambda: q_c(j, hf).wait_send())
    for i, u in spots:
        own = (zq == i) & (tl * nth + u == t)
        pl.when(jnp.logical_not(own))(lambda: at_c(i, u).wait_send())
    kv_out(lambda c: c.wait_send())

    @pl.when(entry)
    def _():
        kv_y0().wait_send()
        kv_s0().wait_send()
        each(1, nz, lambda k: kv_y(k).wait_send())
        each(1, nz, lambda k: kv_s(k, 0).wait_send())
        each(0, nz, lambda k: kv_s(k, 1).wait_send())

    lam_c().wait_send()
    up_y0().wait_send()
    dn_y0().wait_send()
    ow_s0().wait_send()
    h_s0().wait_send()
    sib_c().wait_send()
    for first, last, fns in (
        (1, nz, (up_z, up_y, dn_z, dn_y)),
        (1, nth, (ow_x, ow_s)),
        (1, ntp, (st_c,)),
        (1, ng, (h_p, h_s, red_c)),
    ):
        each(first, last, lambda k: [f(k).wait_send() for f in fns])


def local(nsp, ntp, q1, q2, k1, k2, vals, lam, hg, stream, ow, g1, up, dn, g2):
    tok = q1.shape[0]
    heads = lam.shape[0]
    hv = vals.shape[1]
    vd = hv // heads
    d = ow.shape[1]
    nz, nth = nsp // 2, ntp // 2
    ng = 2 * nth
    share = tok // ntp
    fh = up.shape[1] // 2
    qk = q1.shape[1] // heads
    parts = [a.reshape(tok, heads, -1) for a in (q1, q2, k1, k2, vals)]
    qkv = jnp.concatenate(parts, axis=2).transpose(1, 0, 2)
    nzb, tall = 2 * heads, nth * share
    lam = jnp.broadcast_to(lam[:, None, None], (heads, 1, 128))
    vm = pl.BlockSpec(memory_space=pltpu.VMEM)
    anys = pl.BlockSpec(memory_space=pl.ANY)
    sem = lambda n: pltpu.SemaphoreType.DMA((2, n))
    return pl.pallas_call(
        functools.partial(kernel, nsp, ntp, heads),
        out_shape=jax.ShapeDtypeStruct((share, d), BF16),
        in_specs=[vm, vm, vm, vm, anys, vm, anys, anys, vm],
        out_specs=vm,
        scratch_shapes=[
            pltpu.VMEM((2,) + lam.shape, F32),
            pltpu.VMEM((nzb, tall, 2 * qk), BF16),
            pltpu.VMEM((2, nzb * tall, 2 * qk), BF16),
            pltpu.VMEM((2, 1, nzb * tall), F32),
            pltpu.VMEM((2, 1, nzb * tall), F32),
            pltpu.VMEM((2, vd, nzb * tall), F32),
            pltpu.VMEM((nsp, tok, 2 * qk + vd), BF16),
            pltpu.VMEM((nsp, up.shape[0], fh), BF16),
            pltpu.VMEM((nsp, fh, dn.shape[1]), BF16),
            pltpu.VMEM((ntp,) + ow.shape, BF16),
            pltpu.VMEM((ntp, share, stream.shape[1]), BF16),
            pltpu.VMEM((nzb * tall, vd), BF16),
            pltpu.VMEM((share, ntp * hv), BF16),
            pltpu.VMEM((share, d), F32),
            pltpu.VMEM((share, d), BF16),
            pltpu.VMEM((2, ng, share, d), BF16),
            pltpu.VMEM((2, ng * share, fh), BF16),
            pltpu.VMEM((ng * share, d), BF16),
            pltpu.VMEM((ng * share, d), BF16),
            pltpu.VMEM((ng * share, d), F32),
            pltpu.VMEM((ng, share, d), BF16),
            pltpu.VMEM((ng, share, d), BF16),
            pltpu.SemaphoreType.DMA((3,)),
            sem(1),
            sem(max(2 * heads, nzb)), sem(nz), sem(nz), sem(2 * nz), sem(nz), sem(nz), sem(nz), sem(nz),
            sem(nth), sem(nth), sem(ntp), sem(max(nzb * nth, nzb * nth)), sem(ng), sem(ng), sem(1), sem(ng),
        ],
        compiler_params=pltpu.CompilerParams(
            collective_id=0, has_side_effects=True, vmem_limit_bytes=60 * 1024 * 1024
        ),
    )(lam, qkv, hg.reshape(1, vd), stream, ow, g1.reshape(1, d), up, dn, g2.reshape(1, d))


def solution(mesh):
    in_specs = (
        P("sp", "tp"),
        P("sp", "tp"),
        P("sp", "tp"),
        P("sp", "tp"),
        P("sp", "tp"),
        P("tp"),
        P(),
        P("sp", "tp"),
        P("tp", None),
        P(),
        P("sp", "tp"),
        P("tp", "sp"),
        P(),
    )
    body = functools.partial(local, mesh.shape["sp"], mesh.shape["tp"])
    return jax.shard_map(
        body, mesh=mesh, in_specs=in_specs, out_specs=P(("sp", "tp"), None), check_vma=False
    )
```

profile of v0, /device:TPU:0, one launch (start us, length us, event | category | flops | bytes accessed | tf_op | source)
XLA Modules:
  0.0 114.0 jit_solution(5069914157509646557)
XLA Ops:
  0.0 1.0 copy.18
  1.0 0.0 copy-start
  1.0 0.1 copy.23
  1.1 0.7 copy-done
  1.9 0.1 copy.14
  2.0 0.0 copy-start.1
  2.0 0.1 copy.19
  2.1 0.7 copy-done.1
  2.8 0.1 copy.15
  2.9 0.0 copy-start.2
  2.9 0.1 copy.20
  3.1 0.7 copy-done.2
  3.8 0.1 copy.16
  3.9 0.0 copy-start.3
  3.9 0.1 copy.21
  4.0 0.7 copy-done.3
  4.7 0.1 copy.17
  4.8 0.1 copy.22
  5.0 1.0 concatenate.3
  6.0 0.0 copy-start.4
  6.0 0.7 copy-done.4
  6.6 0.6 broadcast_in_dim.2.lam_ref
  7.2 105.1 %shard_map.127 = bf16[64,2048]{1,0:T(8,128)(2,1)} custom-call(f32[2,1,128]{2,1,0:T(1,128)} %broadcast_in_dim.2.lam_ref, bf16[2,256,384]{2,1,0:T(8,128)(2,1)} %bitcast.9, f32[1,128]{1,0:T(1,128)} %bitcast.17, bf16[256,512]{1,0:T(8,128)(2,1)} %st_ref.1, bf16[256,2048]{1,0:T(8,128)(2,1)} %ow_ref.1, f32[1,2048]{1,0:T(1,128)} %bitcast.15, ...), custom_call_target="tpu_custom_call" | custom-call | tf_op jit(solution)/shard_map/pallas_call | solution.py:467
  112.3 1.7 %copy.25 = bf16[64,2048]{1,0:T(8,128)(2,1)} copy(bf16[64,2048]{1,0:T(8,128)(2,1)} %shard_map.127) | data formatting | bytes 524288
Async XLA Ops:
  1.0 0.8 copy-start
  2.0 0.8 copy-start.1
  2.9 0.8 copy-start.2
  3.9 0.8 copy-start.3
  6.0 0.7 copy-start.4
where the time goes:
time: 114 us
  Pallas kernels  105 us (92%)
  local copies, waits for them, and re-layouts  8.82 us (8%)
    pallas_call x1, Pallas kernels, local(): pl.pallas_call(functools.partial(kernel, nsp, ntp, heads), out_shape=jax....  105 us
    unnamed x16, local copies, waits for them, and re-layouts  6.59 us

commit v1 on v0

v1 whole, which is shorter than its diff:
```python
import functools

import jax
import jax.numpy as jnp
from jax import lax
from jax.experimental import pallas as pl
from jax.experimental.pallas import tpu as pltpu
from jax.sharding import PartitionSpec as P

MESH = pl.DeviceIdType.MESH
F32, BF16 = jnp.float32, jnp.bfloat16
ALPHA = 2.0**0.5
NT = (((1,), (1,)), ((), ()))
TN = (((0,), (0,)), ((), ()))
DIRS = (1, -1)


def layer_norm(value, gain):
    centre = jnp.mean(value, axis=-1, keepdims=True)
    spread = jnp.mean(jnp.square(value - centre), axis=-1, keepdims=True)
    return (value - centre) * lax.rsqrt(spread + 1e-05) * gain


def kernel(
    nsp, ntp, heads,
    lam_ref, q1_ref, q2_ref, k1_ref, k2_ref, v_ref, hg_ref, st_ref, ow_ref, g1_ref, up_ref, dn_ref, g2_ref,
    out_ref,
    lam_all, qin, kin, qsl, slab, hg, g1, g2,
    q_buf, qm, m_run, l_run, acc, kv_buf, up_buf, dn_buf, ow_buf, st_buf, at_snd, at_buf,
    pre, h_own, h_buf, act, sib_snd, sib_buf, part, own_part, red_snd, red_buf,
    loc_sem, lms, gqs, gks, kvr, upr, dnr, upy, dny, owx, ows, sts, ats, hps, hss, sbs, rds,
):
    s, t = lax.axis_index("sp"), lax.axis_index("tp")
    nz, nth = nsp // 2, ntp // 2
    hops = nz // 2
    ng = 2 * nth
    z, y = s // 2, s % 2
    x, c = t // 2, t % 2
    sib_t = x * 2 + (1 - c)
    y_sp = z * 2 + (1 - y)
    grp = y * nth + x
    tok = q1_ref.shape[0]
    share = tok // ntp
    fh = up_ref.shape[1] // 2
    vd = acc.shape[1]
    qw = q_buf.shape[2]
    qk = qw // 2
    d = pre.shape[1]
    out_w = dn_buf.shape[2]
    head_t = x * 2 + y

    def rc(src, dst, sems, i, sp, tp, arrive=None):
        arrive = i if arrive is None else arrive
        return pltpu.make_async_remote_copy(
            src_ref=src, dst_ref=dst, send_sem=sems.at[0, i], recv_sem=sems.at[1, arrive],
            device_id={"sp": sp, "tp": tp}, device_id_type=MESH,
        )

    def each(lo, hi, body):
        if hi - lo <= 4:
            for k in range(lo, hi):
                body(k)
        else:
            lax.fori_loop(lo, hi, lambda k, carry: (body(k), carry)[1], 0)

    def zat(off):
        return lax.rem(z + 2 * nz + off, nz)

    def lc(src, dst, i):
        return pltpu.make_async_copy(src, dst, loc_sem.at[i])

    def up_half(j):
        return up_ref.at[:, pl.ds(pl.multiple_of(j * fh, fh), fh)]

    def dn_half(j):
        return dn_ref.at[pl.ds(pl.multiple_of(j * fh, fh), fh), :]

    def rows_of(tt):
        return pl.ds(pl.multiple_of(tt * share, share), share)

    qk_loads = [
        lc(q1_ref, qin.at[0], 0),
        lc(q2_ref, qin.at[1], 1),
        lc(k1_ref, kin.at[0], 2),
        lc(k2_ref, kin.at[1], 3),
    ]
    v_loads = [
        lc(v_ref.at[:, pl.ds(j * vd, vd)], slab.at[j, :, pl.ds(qw, vd)], 4 + j) for j in range(heads)
    ]
    n0 = 4 + heads
    gain_loads = [lc(hg_ref, hg, n0), lc(g1_ref, g1, n0 + 1), lc(g2_ref, g2, n0 + 2)]
    up_load = lc(up_half(y), up_buf.at[s], n0 + 3)
    dn_load = lc(dn_half(y), dn_buf.at[s], n0 + 4)
    ow_load = lc(ow_ref, ow_buf.at[t], n0 + 5)
    st_load = lc(st_ref.at[rows_of(t), :], st_buf.at[t], n0 + 6)
    for ld in qk_loads + v_loads:
        ld.start()

    def half_of(dr):
        return 0 if dr > 0 else 1

    def piece(buf, origin, side, hf):
        r2 = buf.shape[1] // 2
        return buf.at[origin * 2 + lax.rem(y + side, 2), pl.ds(hf * r2, r2)]

    def slot(dr, k, side, hf):
        return (half_of(dr) * hops + (k - 1)) * 4 + side * 2 + hf

    def ring(item, dr, k, side, hf):
        buf, sems = item
        ref = piece(buf, zat(-dr * (k - 1)), side, hf)
        return rc(ref, ref, sems, slot(dr, k, side, hf), zat(dr) * 2 + y, t)

    def ring_in(item, dr, k, side, hf):
        buf, sems = item
        ref = piece(buf, zat(-dr * k), side, hf)
        return rc(ref, ref, sems, slot(dr, k, side, hf), zat(dr) * 2 + y, t)

    def halves(dr, last=False):
        first = half_of(dr)
        return (first,) if last else (first, 1 - first)

    def ring_first(item, side):
        for n in range(2):
            for dr in DIRS:
                ring(item, dr, 1, side, halves(dr)[n]).start()

    def relay(item, dr, k, side):
        hf = half_of(dr)
        ring_in(item, dr, k, side, hf).wait_recv()
        ring(item, dr, k + 1, side, hf).start()
        if hops > 2:
            @pl.when(k < hops - 1)
            def _():
                ring_in(item, dr, k, side, 1 - hf).wait_recv()
                ring(item, dr, k + 1, side, 1 - hf).start()

    def rest(item, dr, k, side):
        hf = 1 - half_of(dr)
        if hops > 2:
            pl.when(k == hops - 1)(lambda: ring_in(item, dr, k, side, hf).wait_recv())
        else:
            ring_in(item, dr, k, side, hf).wait_recv()

    def last_in(item, side):
        for dr in DIRS:
            ring_in(item, dr, hops, side, half_of(dr)).wait_recv()

    def relay_all(item, side):
        each(1, hops, lambda k: [relay(item, dr, k, side) for dr in DIRS])

    def ring_sent(item):
        def one(k):
            for dr in DIRS:
                for side in range(2):
                    for hf in range(2):
                        if hf == half_of(dr):
                            ring(item, dr, k, side, hf).wait_send()
                        else:
                            ring(item, dr, k, side, hf).wait_send()

        each(1, hops, one)
        for dr in DIRS:
            for side in range(2):
                ring(item, dr, hops, side, half_of(dr)).wait_send()

    kv_item, up_item, dn_item = (kv_buf, kvr), (up_buf, upr), (dn_buf, dnr)

    def lam_c():
        return rc(lam_all.at[c], lam_all.at[c], lms, 0, s, sib_t)

    def q_c(j):
        return rc(qsl.at[j], q_buf.at[y], gqs, j, z * 2 + c, x * 2 + j, y)

    def q_in(side):
        yy = lax.rem(y + side, 2)
        return rc(q_buf.at[yy], q_buf.at[yy], gqs, 0, y_sp, t, yy)

    def kv_c(j):
        return rc(slab.at[j], kv_buf.at[s], gks, j, z * 2 + c, x * 2 + j, y)

    def kv_in(side):
        yy = lax.rem(y + side, 2)
        ref = kv_buf.at[z * 2 + yy]
        return rc(ref, ref, gks, 0, y_sp, t, yy)

    def to_self(j):
        return (c == y) & (c == j)

    def up_y():
        return rc(up_half(1 - y), up_buf.at[s], upy, 0, y_sp, t)

    def dn_y():
        return rc(dn_half(1 - y), dn_buf.at[s], dny, 0, y_sp, t)

    def y_in(buf, sems):
        ref = buf.at[y_sp]
        return rc(ref, ref, sems, 0, y_sp, t)

    def ow_x(k):
        return rc(ow_ref, ow_buf.at[t], owx, k, s, lax.rem(x + k, nth) * 2 + c)

    def ow_s0():
        return rc(ow_ref, ow_buf.at[t], ows, 0, s, sib_t)

    def ow_s(k):
        b = lax.rem(x + nth - k, nth) * 2 + c
        return rc(ow_buf.at[b], ow_buf.at[b], ows, k, s, sib_t)

    def st_c(k):
        td = lax.rem(t + k, ntp)
        return rc(st_ref.at[rows_of(td), :], st_buf.at[t], sts, k, s, td)

    def at_cols():
        return pl.ds(pl.multiple_of(c * vd, vd), vd)

    def at_c(yy, tt):
        rows = pl.ds((yy * ntp + tt) * share, share)
        return rc(
            at_snd.at[rows, :], at_buf.at[head_t, :, at_cols()], ats, yy * ntp + tt,
            z * 2 + yy, tt, head_t * 2 + c,
        )

    def at_in(hd):
        ref = at_buf.at[hd // 2, :, pl.ds((hd % 2) * vd, vd)]
        return rc(ref, ref, ats, 0, y_sp, t, hd)

    def grp_dev(g):
        return z * 2 + g // nth, lax.rem(g, nth) * 2 + c

    def h_p(k):
        sp, tp = grp_dev(lax.rem(grp + k, ng))
        return rc(h_own, h_buf.at[c, grp], hps, k, sp, tp)

    def h_s0():
        return rc(h_own, h_buf.at[c, grp], hss, 0, s, sib_t)

    def h_s(k):
        g = lax.rem(grp + ng - k, ng)
        return rc(h_buf.at[c, g], h_buf.at[c, g], hss, k, s, sib_t)

    def sib_c(zz):
        return rc(sib_snd.at[zz], sib_buf.at[zz], sbs, zz, s, sib_t)

    def red_c(zz, k):
        g = lax.rem(grp + k, ng)
        sp, tp = grp_dev(g)
        return rc(red_snd.at[zz, g], red_buf.at[zz, grp], rds, zz * ng + k, sp, tp)

    barrier = pltpu.get_barrier_semaphore()

    def greet(sp, tp):
        pl.semaphore_signal(barrier, inc=1, device_id={"sp": sp, "tp": tp}, device_id_type=MESH)

    for k in range(1, 2 * ntp):
        o = lax.rem(y * ntp + t + k, 2 * ntp)
        greet(z * 2 + o // ntp, lax.rem(o, ntp))
    for dr in DIRS:
        greet(zat(dr) * 2 + y, t)

    for ld in qk_loads:
        ld.wait()
    for j in range(heads):
        at = slice(j * qk, (j + 1) * qk)
        qsl[j] = jnp.concatenate([qin[0, :, at], qin[1, :, at]], axis=1)
        slab[j, :, :qw] = jnp.concatenate([kin[0, :, at], kin[1, :, at]], axis=1)
        lam_all[c, j] = jnp.full(lam_all.shape[2:], lam_ref[0, j], F32)
    for ld in v_loads:
        ld.wait()
    pl.semaphore_wait(barrier, 2 * ntp - 1 + 2)

    for j in range(heads):
        pl.when(jnp.logical_not(to_self(j)))(lambda: q_c(j).start())
    for j in range(heads):
        pl.when(jnp.logical_not(to_self(j)))(lambda: kv_c(j).start())
    for j in range(heads):
        @pl.when(to_self(j))
        def _():
            q_buf[y] = qsl[j]
            kv_buf[s] = slab[j]

    lam_c().start()
    up_y().start()
    each(1, ntp, lambda k: st_c(k).start())
    each(1, nth, lambda k: ow_x(k).start())
    ow_s0().start()
    dn_y().start()
    for ld in gain_loads + [st_load, ow_load, up_load, dn_load]:
        ld.start()

    m_run[...] = jnp.full(m_run.shape, -1e30, F32)
    l_run[...] = jnp.zeros(l_run.shape, F32)
    acc[...] = jnp.zeros(acc.shape, F32)

    pl.when(c != y)(lambda: kv_in(0).wait_recv())
    ring_first(kv_item, 0)
    pl.when(c != y)(lambda: q_in(0).wait_recv())
    q_in(1).wait_recv()
    scale = qk ** (-0.5)
    lane = lax.broadcasted_iota(jnp.int32, (tok, qw), 1)
    for i in range(2):
        qv = q_buf[i].astype(F32) * scale
        for mp in range(2):
            keep = (lane >= mp * qk) & (lane < (mp + 1) * qk)
            qm[mp, i * tok : (i + 1) * tok, :] = jnp.where(keep, qv, 0.0).astype(BF16)

    def absorb(block):
        v = block[:, qw:]
        for r in range(2):
            sc = lax.dot_general(block[:, :qw], qm[r], NT, preferred_element_type=F32)
            old = m_run[r]
            new = jnp.maximum(old, jnp.max(sc, axis=0, keepdims=True))
            fac = jnp.exp(old - new)
            ex = jnp.exp(sc - new)
            l_run[r] = l_run[r] * fac + jnp.sum(ex, axis=0, keepdims=True)
            acc[r] = acc[r] * fac + lax.dot_general(
                v, ex.astype(BF16), TN, preferred_element_type=F32
            )
            m_run[r] = new

    def own_up(side):
        if side == 0:
            r2 = up_ref.shape[0] // 2
            for n in range(2):
                for dr in DIRS:
                    own_first(up_ref, up_item, dr, halves(dr)[n], r2).start()
        else:
            y_in(up_buf, upy).wait_recv()
            ring_first(up_item, 1)

    def own_first(ref, item, dr, hf, r2):
        buf, sems = item
        if ref is up_ref:
            src = up_ref.at[pl.ds(hf * r2, r2), pl.ds(pl.multiple_of(y * fh, fh), fh)]
        else:
            src = dn_ref.at[pl.ds(pl.multiple_of(y * fh + hf * r2, r2), r2), :]
        return rc(src, buf.at[s, pl.ds(hf * r2, r2)], sems, slot(dr, 1, 0, hf), zat(dr) * 2 + y, t)

    def own_dn(side):
        if side == 0:
            r2 = fh // 2
            for n in range(2):
                for dr in DIRS:
                    own_first(dn_ref, dn_item, dr, halves(dr)[n], r2).start()
        else:
            y_in(dn_buf, dny).wait_recv()
            ring_first(dn_item, 1)

    def step(i, carry):
        k = (i + 2) // 4
        r = lax.rem(i + 2, 4)
        mid = (k > 0) & (k < hops)

        @pl.when(i == 1)
        def _():
            pl.when(jnp.bool_(True))(lambda: kv_in(1).wait_recv())
            ring_first(kv_item, 1)

        for side in range(2):
            @pl.when(mid & (r == 2 * side))
            def _():
                for dr in DIRS:
                    relay(kv_item, dr, k, side)
                rest(kv_item, 1, k, side)

            @pl.when(mid & (r == 2 * side + 1))
            def _():
                rest(kv_item, -1, k, side)

            @pl.when((k == hops) & (r == side))
            def _():
                last_in(kv_item, side)

        @pl.when(i == 4 * hops - 4)
        def _():
            own_up(0)
            own_up(1)

        side = jnp.where(k == 0, r - 2, jnp.where(k == hops, r, r // 2))
        off = jnp.where(mid & (lax.rem(r, 2) == 1), k, -k)
        absorb(kv_buf.at[zat(off) * 2 + lax.rem(y + side, 2)])
        return carry

    lax.fori_loop(0, 2 * nz, step, 0)

    for ld in gain_loads:
        ld.wait()
    lam_c().wait_recv()
    lam = lam_all[y, c][:, :1]
    mixed = acc[0] / l_run[0] - lam * (acc[1] / l_run[1])
    inv = lax.rsqrt(jnp.mean(jnp.square(mixed), axis=0, keepdims=True) + 1e-05)
    normed = jnp.transpose(mixed * inv) * hg[...] * 0.8
    at_snd[...] = normed.astype(BF16)
    spots = [(yy, tt) for yy in range(2) for tt in range(ntp)]
    for yy, tt in spots:
        mine = (yy == y) & (tt == t)
        pl.when(jnp.logical_not(mine))(lambda: at_c(yy, tt).start())

        @pl.when(mine)
        def _():
            n = (yy * ntp + tt) * share
            at_buf[head_t, :, at_cols()] = at_snd[n : n + share, :]

    relay_all(up_item, 0)
    own_dn(0)
    relay_all(up_item, 1)
    own_dn(1)

    for k in range(1, nth):
        ow_x(k).wait_recv()
        ow_s(k).start()
    st_load.wait()
    each(1, ntp, lambda k: st_c(k).wait_recv())
    cols = st_ref.shape[1]
    for b in range(ntp):
        pre[:, b * cols : (b + 1) * cols] = ALPHA * st_buf[b].astype(F32)
    for hd in range(2 * ntp):
        pl.when(head_t * 2 + c != hd)(lambda: at_in(hd).wait_recv())
    ow_load.wait()
    ow_s0().wait_recv()
    for k in range(1, nth):
        ow_s(k).wait_recv()
    for b in range(ntp):
        at = slice(b * cols, (b + 1) * cols)
        tot = pre[:, at]
        for tt in range(ntp):
            tot += jnp.dot(at_buf[tt], ow_buf[tt, :, at], preferred_element_type=F32)
        pre[:, at] = tot
    h_own[...] = layer_norm(pre[...], g1[...]).astype(BF16)
    each(1, ng, lambda k: h_p(k).start())
    h_s0().start()
    h_buf[c, grp] = h_own[...]

    def h_fwd(k):
        h_p(k).wait_recv()
        h_s(k).start()

    each(1, ng, h_fwd)
    relay_all(dn_item, 0)
    up_load.wait()
    for side in range(2):
        each(1, hops, lambda k: [rest(up_item, dr, k, side) for dr in DIRS])
        last_in(up_item, side)
    h_s0().wait_recv()
    each(1, ng, lambda k: h_s(k).wait_recv())

    half = ng * share
    for side in range(2):
        parts = 2 if fh % 256 == 0 else 1
        for n in range(parts):
            wide = fh // parts
            at = slice(n * wide, (n + 1) * wide)
            hid = h_buf[side].reshape(half, d)
            w = up_buf[:, :, at].reshape(d, wide)
            up = jnp.dot(hid, w, preferred_element_type=F32)
            act[side, :, at] = jnp.square(jnp.maximum(up, 0.0)).astype(BF16)

    dn_load.wait()

    def unit(u):
        k = (u + 1) // 2
        return k, zat(jnp.where((lax.rem(u, 2) == 0) & (k < hops), k, -k))

    def finish(u):
        zz = unit(u)[1]
        sib_c(zz).wait_recv()
        for k in range(ng - 1, 0, -1):
            g = lax.rem(grp + k, ng)
            rows = pl.ds(pl.multiple_of(g * share, share), share)
            red_snd[zz, g] = (part[zz, :, rows, :] + sib_buf[zz, :, rows, :].astype(F32)).astype(BF16)
            red_c(zz, k).start()
        rows = pl.ds(pl.multiple_of(grp * share, share), share)
        own_part[zz] = part[zz, :, rows, :] + sib_buf[zz, :, rows, :].astype(F32)

    def down(u, carry):
        k, zz = unit(u)

        @pl.when(u == 1)
        def _():
            relay_all(dn_item, 1)

        @pl.when((k > 0) & (k < hops))
        def _():
            for dr in DIRS:
                @pl.when(lax.rem(u, 2) == (1 if dr > 0 else 0))
                def _():
                    for side in range(2):
                        rest(dn_item, dr, k, side)

        @pl.when(k == hops)
        def _():
            for side in range(2):
                last_in(dn_item, side)

        for yy in range(2):
            res = jnp.dot(act[1 - c], dn_buf[zz * 2 + yy], preferred_element_type=F32)
            sib_snd[zz, yy] = res.astype(BF16)
        sib_c(zz).start()
        for yy in range(2):
            part[zz, yy] = jnp.dot(act[c], dn_buf[zz * 2 + yy], preferred_element_type=F32)
        pl.when(u > 0)(lambda: finish(u - 1))
        return carry

    lax.fori_loop(0, nz, down, 0)
    finish(nz - 1)

    for zz in range(nz):
        for k in range(1, ng):
            red_c(zz, k).wait_recv()
        for yy in range(2):
            at = slice((zz * 2 + yy) * out_w, (zz * 2 + yy + 1) * out_w)
            tot = own_part[zz, yy] + ALPHA * h_own[:, at].astype(F32)
            for k in range(ng - 1, 0, -1):
                tot += red_buf[zz, lax.rem(grp + ng - k, ng), yy].astype(F32)
            pre[:, at] = tot
    out_ref[...] = layer_norm(pre[...], g2[...]).astype(BF16)

    for j in range(heads):
        @pl.when(jnp.logical_not(to_self(j)))
        def _():
            q_c(j).wait_send()
            kv_c(j).wait_send()

    for yy, tt in spots:
        mine = (yy == y) & (tt == t)
        pl.when(jnp.logical_not(mine))(lambda: at_c(yy, tt).wait_send())
    for item in (kv_item, up_item, dn_item):
        ring_sent(item)
    lam_c().wait_send()
    up_y().wait_send()
    dn_y().wait_send()
    ow_s0().wait_send()
    h_s0().wait_send()
    each(0, nz, lambda zz: [sib_c(zz).wait_send()] + [red_c(zz, k).wait_send() for k in range(1, ng)])
    for first, last, fns in ((1, nth, (ow_x, ow_s)), (1, ntp, (st_c,)), (1, ng, (h_p, h_s))):
        each(first, last, lambda k: [f(k).wait_send() for f in fns])


def local(nsp, ntp, q1, q2, k1, k2, vals, lam, hg, stream, ow, g1, up, dn, g2):
    tok = q1.shape[0]
    heads = lam.shape[0]
    hv = vals.shape[1]
    vd = hv // heads
    d = ow.shape[1]
    nz, nth = nsp // 2, ntp // 2
    ng = 2 * nth
    share = tok // ntp
    fh = up.shape[1] // 2
    qk = q1.shape[1] // heads
    half, out_w = ng * share, dn.shape[1]
    vm = pl.BlockSpec(memory_space=pltpu.VMEM)
    sm = pl.BlockSpec(memory_space=pltpu.SMEM)
    hbm = pl.BlockSpec(memory_space=pl.ANY)
    sem = lambda n: pltpu.SemaphoreType.DMA((2, n))
    return pl.pallas_call(
        functools.partial(kernel, nsp, ntp, heads),
        out_shape=jax.ShapeDtypeStruct((share, d), BF16),
        in_specs=[sm] + [hbm] * 12,
        out_specs=vm,
        scratch_shapes=[
            pltpu.VMEM((2, heads, 1, 128), F32),
            pltpu.VMEM((2, tok, heads * qk), BF16),
            pltpu.VMEM((2, tok, heads * qk), BF16),
            pltpu.VMEM((heads, tok, 2 * qk), BF16),
            pltpu.VMEM((heads, tok, 2 * qk + vd), BF16),
            pltpu.VMEM((1, vd), F32),
            pltpu.VMEM((1, d), F32),
            pltpu.VMEM((1, d), F32),
            pltpu.VMEM((2, tok, 2 * qk), BF16),
            pltpu.VMEM((2, 2 * tok, 2 * qk), BF16),
            pltpu.VMEM((2, 1, 2 * tok), F32),
            pltpu.VMEM((2, 1, 2 * tok), F32),
            pltpu.VMEM((2, vd, 2 * tok), F32),
            pltpu.VMEM((nsp, tok, 2 * qk + vd), BF16),
            pltpu.VMEM((nsp, up.shape[0], fh), BF16),
            pltpu.VMEM((nsp, fh, out_w), BF16),
            pltpu.VMEM((ntp,) + ow.shape, BF16),
            pltpu.VMEM((ntp, share, stream.shape[1]), BF16),
            pltpu.VMEM((2 * tok, vd), BF16),
            pltpu.VMEM((ntp, share, hv), BF16),
            pltpu.VMEM((share, d), F32),
            pltpu.VMEM((share, d), BF16),
            pltpu.VMEM((2, ng, share, d), BF16),
            pltpu.VMEM((2, half, fh), BF16),
            pltpu.VMEM((nz, 2, half, out_w), BF16),
            pltpu.VMEM((nz, 2, half, out_w), BF16),
            pltpu.VMEM((nz, 2, half, out_w), F32),
            pltpu.VMEM((nz, 2, share, out_w), F32),
            pltpu.VMEM((nz, ng, 2, share, out_w), BF16),
            pltpu.VMEM((nz, ng, 2, share, out_w), BF16),
            pltpu.SemaphoreType.DMA((4 + heads + 7,)),
            sem(1), sem(heads), sem(heads), sem(4 * nz), sem(4 * nz), sem(4 * nz), sem(1), sem(1),
            sem(nth), sem(nth), sem(ntp), sem(2 * ntp), sem(ng), sem(ng), sem(nz), sem(nz * ng),
        ],
        compiler_params=pltpu.CompilerParams(
            collective_id=0, has_side_effects=True, vmem_limit_bytes=60 * 1024 * 1024
        ),
    )(
        lam.reshape(1, heads), q1, q2, k1, k2, vals, hg.reshape(1, vd), stream, ow,
        g1.reshape(1, d), up, dn, g2.reshape(1, d),
    )


def solution(mesh):
    in_specs = (
        P("sp", "tp"),
        P("sp", "tp"),
        P("sp", "tp"),
        P("sp", "tp"),
        P("sp", "tp"),
        P("tp"),
        P(),
        P("sp", "tp"),
        P("tp", None),
        P(),
        P("sp", "tp"),
        P("tp", "sp"),
        P(),
    )
    body = functools.partial(local, mesh.shape["sp"], mesh.shape["tp"])
    return jax.shard_map(
        body, mesh=mesh, in_specs=in_specs, out_specs=P(("sp", "tp"), None), check_vma=False
    )
```

time: 114 us -> 106 us (0.930)
  local copies, waits for them, and re-layouts: 8.82 us -> 1.67 us
    unnamed x16 -> x1, local copies, waits for them, and re-layouts: 6.59 us -> 1.67 us
    pallas_call x1, Pallas kernels: 105 us -> 104 us  [local(): pl.pallas_call(functools.partial(kernel, nsp, ntp, heads), out_shape=jax....]
where the time goes in v1:
time: 106 us
  Pallas kernels  104 us (98%)
  local copies, waits for them, and re-layouts  1.67 us (2%)
    pallas_call x1, Pallas kernels, local(): pl.pallas_call(functools.partial(kernel, nsp, ntp, heads), out_shape=jax....  104 us

profile of v1, /device:TPU:0, one launch (start us, length us, event | category | flops | bytes accessed | tf_op | source)
XLA Modules:
  0.0 105.6 jit_solution(13995194962336661687)
XLA Ops:
  0.0 103.9 %shard_map.127 = bf16[64,2048]{1,0:T(8,128)(2,1)} custom-call(f32[1,2]{1,0:T(1,128)} %bitcast.6, bf16[256,128]{1,0:T(8,128)(2,1)} %q1_ref.1, bf16[256,128]{1,0:T(8,128)(2,1)} %q2_ref.1, bf16[256,128]{1,0:T(8,128)(2,1)} %k1_ref.1, bf16[256,128]{1,0:T(8,128)(2,1)} %k2_ref.1, bf16[256,256]{1,0:T(8,128)(2,1)} %v_ref.1, f32[1,128]{1,0:T(1,128)} %bitcast.7, ...), custom_call_target="tpu_custom_call" | custom-call | tf_op jit(solution)/shard_map/pallas_call | solution.py:555
  103.9 1.7 %copy.15 = bf16[64,2048]{1,0:T(8,128)(2,1)} copy(bf16[64,2048]{1,0:T(8,128)(2,1)} %shard_map.127) | data formatting | bytes 524288

commit v2 on v1

v2 whole, which is shorter than its diff:
```python
import functools

import jax
import jax.numpy as jnp
from jax import lax
from jax.experimental import pallas as pl
from jax.experimental.pallas import tpu as pltpu
from jax.sharding import PartitionSpec as P

MESH = pl.DeviceIdType.MESH
F32, BF16 = jnp.float32, jnp.bfloat16
ALPHA = 2.0**0.5
NT = (((1,), (1,)), ((), ()))
TN = (((0,), (0,)), ((), ()))


def layer_norm(value, gain):
    centre = jnp.mean(value, axis=-1, keepdims=True)
    spread = jnp.mean(jnp.square(value - centre), axis=-1, keepdims=True)
    return (value - centre) * lax.rsqrt(spread + 1e-05) * gain


def kernel(
    nsp, ntp, heads, pieces,
    lam_ref, q1_ref, q2_ref, k1_ref, k2_ref, v_ref, hg_ref, st_ref, ow_ref, g1_ref, up_ref, dn_ref, g2_ref,
    out_ref,
    lam_all, qin, kin, qsl, slab, hg, g1, g2,
    q_buf, qm, m_run, l_run, acc, kv_buf, up_buf, dn_buf, ow_buf, st_buf, at_snd, at_buf,
    pre, h_own, h_buf, act, sib_snd, sib_buf, part, own_part, red_snd, red_buf,
    loc_sem, lms, gqs, kvd, kvs, upz, upy, dnz, dny, owx, ows, sts, ats, hps, hss, sbs, rds,
):
    s, t = lax.axis_index("sp"), lax.axis_index("tp")
    nz, nth = nsp // 2, ntp // 2
    npair = nz // 2
    ng = 2 * nth
    z, y = s // 2, s % 2
    zh, zl = z // 2, z % 2
    mate = zh * 2 + 1 - zl
    x, c = t // 2, t % 2
    sib_t = x * 2 + (1 - c)
    y_sp = z * 2 + (1 - y)
    grp = zl * nth + x
    tok = q1_ref.shape[0]
    share = tok // ntp
    fh = up_ref.shape[1] // 2
    vd = acc.shape[1]
    qw = q_buf.shape[2]
    qk = qw // 2
    d = pre.shape[1]
    out_w = dn_buf.shape[2]
    pw = out_w // pieces
    head_t = x * 2 + zl

    def rc(src, dst, sems, i, sp, tp, arrive=None):
        arrive = i if arrive is None else arrive
        return pltpu.make_async_remote_copy(
            src_ref=src, dst_ref=dst, send_sem=sems.at[0, i], recv_sem=sems.at[1, arrive],
            device_id={"sp": sp, "tp": tp}, device_id_type=MESH,
        )

    def each(lo, hi, body):
        if hi - lo <= 4:
            for k in range(lo, hi):
                body(k)
        else:
            lax.fori_loop(lo, hi, lambda k, carry: (body(k), carry)[1], 0)

    def lc(src, dst, i):
        return pltpu.make_async_copy(src, dst, loc_sem.at[i])

    def up_half(j):
        return up_ref.at[:, pl.ds(pl.multiple_of(j * fh, fh), fh)]

    def dn_rows(j):
        return pl.ds(pl.multiple_of(j * fh, fh), fh)

    def rows_of(tt):
        return pl.ds(pl.multiple_of(tt * share, share), share)

    qk_loads = [
        lc(q1_ref, qin.at[0], 0),
        lc(q2_ref, qin.at[1], 1),
        lc(k1_ref, kin.at[0], 2),
        lc(k2_ref, kin.at[1], 3),
    ]
    v_loads = [
        lc(v_ref.at[:, pl.ds(j * vd, vd)], slab.at[j, :, pl.ds(qw, vd)], 4 + j) for j in range(heads)
    ]
    n0 = 4 + heads
    gain_loads = [lc(hg_ref, hg, n0), lc(g1_ref, g1, n0 + 1), lc(g2_ref, g2, n0 + 2)]
    up_load = lc(up_half(zl), up_buf.at[s], n0 + 3)
    dn_load = lc(dn_ref.at[dn_rows(zl), :], dn_buf.at[s], n0 + 4)
    ow_load = lc(ow_ref, ow_buf.at[t], n0 + 5)
    st_load = lc(st_ref.at[rows_of(t), :], st_buf.at[t], n0 + 6)
    for ld in qk_loads + v_loads:
        ld.start()

    def lam_c():
        return rc(lam_all.at[c], lam_all.at[c], lms, 0, s, sib_t)

    def to_self(j):
        return (c == zl) & (y == c) & (j == y)

    self_worker = (c == zl) & (y == c)

    def q_c(j):
        return rc(qsl.at[j], q_buf.at[zl], gqs, j, (zh * 2 + c) * 2 + j, x * 2 + y, zl)

    def q_in(i):
        return rc(q_buf.at[i], q_buf.at[i], gqs, 0, y_sp, t, i)

    def kv_c(r, j):
        return rc(slab.at[j], kv_buf.at[s], kvd, r * heads + j, (r * 2 + c) * 2 + j, x * 2 + y, z)

    def kv_in(zz):
        ref = kv_buf.at[zz * 2 + c]
        return rc(ref, ref, kvd, 0, y_sp, t, zz)

    def kv_s(zz, side):
        ref = kv_buf.at[zz * 2 + side]
        return rc(ref, ref, kvs, zz, s, sib_t)

    def kv_out(fn, own):
        for j in range(heads):
            if own:
                pl.when(jnp.logical_not(to_self(j)))(lambda: fn(kv_c(zh, j)))
            else:
                each(1, npair, lambda q: fn(kv_c(lax.rem(zh + q, npair), j)))

    def up_z(zz):
        return rc(up_half(zz % 2), up_buf.at[s], upz, zz, zz * 2 + y, t, z)

    def up_zin(zz):
        ref = up_buf.at[zz * 2 + y]
        return rc(ref, ref, upz, 0, y_sp, t, zz)

    def up_y0():
        return rc(up_half(zl), up_buf.at[s], upy, z, y_sp, t)

    def up_y(zz, side=0):
        ref = up_buf.at[zz * 2 + lax.rem(y + side, 2)]
        return rc(ref, ref, upy, zz, y_sp, t)

    def cols_of(p):
        return pl.ds(p * pw, pw)

    def dn_z(zz, p):
        return rc(
            dn_ref.at[dn_rows(zz % 2), cols_of(p)], dn_buf.at[s, :, cols_of(p)],
            dnz, zz * pieces + p, zz * 2 + y, t, z * pieces + p,
        )

    def dn_zin(zz, p):
        ref = dn_buf.at[zz * 2 + y, :, cols_of(p)]
        return rc(ref, ref, dnz, 0, y_sp, t, zz * pieces + p)

    def dn_y0(p):
        return rc(
            dn_ref.at[dn_rows(zl), cols_of(p)], dn_buf.at[s, :, cols_of(p)], dny, z * pieces + p, y_sp, t
        )

    def dn_y(zz, p, side=0):
        ref = dn_buf.at[zz * 2 + lax.rem(y + side, 2), :, cols_of(p)]
        return rc(ref, ref, dny, zz * pieces + p, y_sp, t)

    def ow_x(k):
        return rc(ow_ref, ow_buf.at[t], owx, k, s, lax.rem(x + k, nth) * 2 + c)

    def ow_s0():
        return rc(ow_ref, ow_buf.at[t], ows, 0, s, sib_t)

    def ow_s(k):
        b = lax.rem(x + nth - k, nth) * 2 + c
        return rc(ow_buf.at[b], ow_buf.at[b], ows, k, s, sib_t)

    def st_c(k):
        td = lax.rem(t + k, ntp)
        return rc(st_ref.at[rows_of(td), :], st_buf.at[t], sts, k, s, td)

    def at_cols():
        return pl.ds(pl.multiple_of(y * vd, vd), vd)

    def at_c(i, tt):
        rows = pl.ds((i * ntp + tt) * share, share)
        return rc(
            at_snd.at[rows, :], at_buf.at[head_t, :, at_cols()], ats, i * ntp + tt,
            (zh * 2 + i) * 2 + c, tt, head_t * 2 + y,
        )

    def at_in(hd):
        ref = at_buf.at[hd // 2, :, pl.ds((hd % 2) * vd, vd)]
        return rc(ref, ref, ats, 0, y_sp, t, hd)

    def grp_dev(g):
        return (zh * 2 + g // nth) * 2 + y, lax.rem(g, nth) * 2 + c

    def h_p(k):
        sp, tp = grp_dev(lax.rem(grp + k, ng))
        return rc(h_own, h_buf.at[c, grp], hps, k, sp, tp)

    def h_s0():
        return rc(h_own, h_buf.at[c, grp], hss, 0, s, sib_t)

    def h_s(k):
        g = lax.rem(grp + ng - k, ng)
        return rc(h_buf.at[c, g], h_buf.at[c, g], hss, k, s, sib_t)

    def sib_c(n):
        return rc(sib_snd.at[n], sib_buf.at[n], sbs, n, s, sib_t)

    def red_c(n, k):
        g = lax.rem(grp + k, ng)
        sp, tp = grp_dev(g)
        return rc(red_snd.at[n, g], red_buf.at[n, grp], rds, n * ng + k, sp, tp)

    def other(q, m):
        r = lax.rem(zh + q, npair)
        return r * 2 + jnp.where(r > zh, m, 1 - m)

    def shared(zz):
        return (zz > z) == (mate > z)

    def others(fn):
        for m in range(2):
            each(1, npair, lambda q: fn(other(q, m)))

    barrier = pltpu.get_barrier_semaphore()

    def greet(sp, tp):
        pl.semaphore_signal(barrier, inc=1, device_id={"sp": sp, "tp": tp}, device_id_type=MESH)

    for o in range(4 * ntp):
        sp, tt = zh * 4 + o // ntp, o % ntp
        pl.when((sp != s) | (tt != t))(functools.partial(greet, sp, tt))

    def greet_far(q):
        for o in range(8):
            greet(lax.rem(zh + q, npair) * 4 + o // 2, x * 2 + o % 2)

    each(1, npair, greet_far)

    for ld in qk_loads:
        ld.wait()
    for j in range(heads):
        at = slice(j * qk, (j + 1) * qk)
        qsl[j] = jnp.concatenate([qin[0, :, at], qin[1, :, at]], axis=1)
        slab[j, :, :qw] = jnp.concatenate([kin[0, :, at], kin[1, :, at]], axis=1)
        lam_all[c, j] = jnp.full(lam_all.shape[2:], lam_ref[0, j], F32)
    for ld in v_loads:
        ld.wait()
    pl.semaphore_wait(barrier, 4 * ntp - 1 + 8 * (npair - 1))

    kv_out(lambda cp: cp.start(), False)
    for j in range(heads):
        pl.when(jnp.logical_not(to_self(j)))(lambda: q_c(j).start())
    kv_out(lambda cp: cp.start(), True)
    for j in range(heads):
        @pl.when(to_self(j))
        def _():
            q_buf[zl] = qsl[j]
            kv_buf[s] = slab[j]

    lam_c().start()
    each(1, ntp, lambda k: st_c(k).start())
    each(1, nth, lambda k: ow_x(k).start())
    ow_s0().start()
    others(lambda zz: up_z(zz).start())
    up_z(mate).start()
    up_y0().start()
    for ld in gain_loads + [st_load, ow_load, up_load, dn_load]:
        ld.start()

    def dn_far(early):
        for p in range(pieces):
            others(lambda zz: pl.when(shared(zz) != early)(lambda: dn_z(zz, p).start()))

    dn_far(True)

    m_run[...] = jnp.full(m_run.shape, -1e30, F32)
    l_run[...] = jnp.zeros(l_run.shape, F32)
    acc[...] = jnp.zeros(acc.shape, F32)
    scale = qk ** (-0.5)
    lane = lax.broadcasted_iota(jnp.int32, (tok, qw), 1)
    for i in range(2):
        pl.when(jnp.logical_not(self_worker & (zl == i)))(lambda: q_in(i).wait_recv())
        qv = q_buf[i].astype(F32) * scale
        for mp in range(2):
            keep = (lane >= mp * qk) & (lane < (mp + 1) * qk)
            qm[mp, i * tok : (i + 1) * tok, :] = jnp.where(keep, qv, 0.0).astype(BF16)

    def absorb(block):
        v = block[:, qw:]
        for r in range(2):
            sc = lax.dot_general(block[:, :qw], qm[r], NT, preferred_element_type=F32)
            old = m_run[r]
            new = jnp.maximum(old, jnp.max(sc, axis=0, keepdims=True))
            fac = jnp.exp(old - new)
            ex = jnp.exp(sc - new)
            l_run[r] = l_run[r] * fac + jnp.sum(ex, axis=0, keepdims=True)
            acc[r] = acc[r] * fac + lax.dot_general(
                v, ex.astype(BF16), TN, preferred_element_type=F32
            )
            m_run[r] = new

    def step(i, carry):
        zz = lax.rem(zh * 2 + i // 2, nz)
        own = lax.rem(i, 2) == 0

        @pl.when(own)
        def _():
            pl.when(jnp.logical_not(self_worker & (zz == z)))(lambda: kv_in(zz).wait_recv())
            kv_s(zz, c).start()

        pl.when(jnp.logical_not(own))(lambda: kv_s(zz, 1 - c).wait_recv())
        absorb(kv_buf.at[zz * 2 + jnp.where(own, c, 1 - c)])
        return carry

    lax.fori_loop(0, nsp, step, 0)

    for ld in gain_loads:
        ld.wait()
    lam_c().wait_recv()
    lam = lam_all[zl, y][:, :1]
    mixed = acc[0] / l_run[0] - lam * (acc[1] / l_run[1])
    inv = lax.rsqrt(jnp.mean(jnp.square(mixed), axis=0, keepdims=True) + 1e-05)
    normed = jnp.transpose(mixed * inv) * hg[...] * 0.8
    at_snd[...] = normed.astype(BF16)
    spots = [(i, tt) for i in range(2) for tt in range(ntp)]

    def at_mine(i, tt):
        return (i == zl) & (y == c) & (tt == t)

    for i, tt in spots:
        pl.when(jnp.logical_not(at_mine(i, tt)))(lambda: at_c(i, tt).start())

        @pl.when(at_mine(i, tt))
        def _():
            n = (i * ntp + tt) * share
            at_buf[head_t, :, at_cols()] = at_snd[n : n + share, :]

    def up_fwd(zz):
        up_zin(zz).wait_recv()
        up_y(zz).start()

    up_fwd(mate)
    for k in range(1, nth):
        ow_x(k).wait_recv()
        ow_s(k).start()
    st_load.wait()
    each(1, ntp, lambda k: st_c(k).wait_recv())
    cols = st_ref.shape[1]
    for b in range(ntp):
        pre[:, b * cols : (b + 1) * cols] = ALPHA * st_buf[b].astype(F32)
    for hd in range(2 * ntp):
        pl.when((y != c) | (head_t * 2 + y != hd))(lambda: at_in(hd).wait_recv())
    ow_load.wait()
    ow_s0().wait_recv()
    for k in range(1, nth):
        ow_s(k).wait_recv()
    for b in range(ntp):
        at = slice(b * cols, (b + 1) * cols)
        tot = pre[:, at]
        for tt in range(ntp):
            tot += jnp.dot(at_buf[tt], ow_buf[tt, :, at], preferred_element_type=F32)
        pre[:, at] = tot
    h_own[...] = layer_norm(pre[...], g1[...]).astype(BF16)
    each(1, ng, lambda k: h_p(k).start())
    h_s0().start()
    dn_far(False)
    for p in range(pieces):
        dn_z(mate, p).start()
    for p in range(pieces):
        dn_y0(p).start()
    h_buf[c, grp] = h_own[...]
    others(up_fwd)

    def h_fwd(k):
        h_p(k).wait_recv()
        h_s(k).start()

    each(1, ng, h_fwd)
    up_load.wait()
    each(0, nz, lambda zz: up_y(zz, 1).wait_recv())
    h_s0().wait_recv()
    each(1, ng, lambda k: h_s(k).wait_recv())

    half = ng * share
    for side in range(2):
        parts = 2 if fh % 256 == 0 else 1
        for n in range(parts):
            wide = fh // parts
            at = slice(n * wide, (n + 1) * wide)
            hid = h_buf[side].reshape(half, d)
            w = up_buf[:, :, at].reshape(d, wide)
            up = jnp.dot(hid, w, preferred_element_type=F32)
            act[side, :, at] = jnp.square(jnp.maximum(up, 0.0)).astype(BF16)

    dn_load.wait()

    def unit(u):
        w = u // pieces
        return jnp.where(w == 0, z, jnp.where(w == 1, mate, other(w // 2, lax.rem(w, 2))))

    def finish(n):
        sib_c(n).wait_recv()
        for k in range(ng - 1, 0, -1):
            g = lax.rem(grp + k, ng)
            rows = pl.ds(pl.multiple_of(g * share, share), share)
            red_snd[n, g] = (part[n, :, rows, :] + sib_buf[n, :, rows, :].astype(F32)).astype(BF16)
            red_c(n, k).start()
        rows = pl.ds(pl.multiple_of(grp * share, share), share)
        own_part[n] = part[n, :, rows, :] + sib_buf[n, :, rows, :].astype(F32)

    def down(w, carry):
        zz = unit(w * pieces)
        before = unit(w * pieces - pieces)
        for p in range(pieces):
            n = zz * pieces + p

            @pl.when(w > 0)
            def _():
                dn_zin(zz, p).wait_recv()
                dn_y(zz, p).start()

            dn_y(zz, p, 1).wait_recv()
            at = slice(p * pw, (p + 1) * pw)
            for yy in range(2):
                res = jnp.dot(act[1 - c], dn_buf[zz * 2 + yy, :, at], preferred_element_type=F32)
                sib_snd[n, yy] = res.astype(BF16)
            sib_c(n).start()
            for yy in range(2):
                part[n, yy] = jnp.dot(act[c], dn_buf[zz * 2 + yy, :, at], preferred_element_type=F32)
            if p > 0:
                finish(n - 1)
            else:
                pl.when(w > 0)(lambda: finish(before * pieces + pieces - 1))
        return carry

    lax.fori_loop(0, nz, down, 0)
    finish(unit(nz * pieces - pieces) * pieces + pieces - 1)

    for zz in range(nz):
        for p in range(pieces):
            n = zz * pieces + p
            for k in range(1, ng):
                red_c(n, k).wait_recv()
            for yy in range(2):
                lo = (zz * 2 + yy) * out_w + p * pw
                at = slice(lo, lo + pw)
                tot = own_part[n, yy] + ALPHA * h_own[:, at].astype(F32)
                for k in range(ng - 1, 0, -1):
                    tot += red_buf[n, lax.rem(grp + ng - k, ng), yy].astype(F32)
                pre[:, at] = tot
    out_ref[...] = layer_norm(pre[...], g2[...]).astype(BF16)

    for j in range(heads):
        pl.when(jnp.logical_not(to_self(j)))(lambda: q_c(j).wait_send())
    kv_out(lambda cp: cp.wait_send(), False)
    kv_out(lambda cp: cp.wait_send(), True)
    for i, tt in spots:
        pl.when(jnp.logical_not(at_mine(i, tt)))(lambda: at_c(i, tt).wait_send())

    def sent(zz):
        up_z(zz).wait_send()
        up_y(zz).wait_send()
        for p in range(pieces):
            dn_z(zz, p).wait_send()
            dn_y(zz, p).wait_send()

    others(sent)
    sent(mate)
    up_y0().wait_send()
    for p in range(pieces):
        dn_y0(p).wait_send()
    each(0, nz, lambda zz: kv_s(zz, c).wait_send())
    lam_c().wait_send()
    ow_s0().wait_send()
    h_s0().wait_send()
    each(0, nz * pieces, lambda n: [sib_c(n).wait_send()] + [red_c(n, k).wait_send() for k in range(1, ng)])
    for first, last, fns in ((1, nth, (ow_x, ow_s)), (1, ntp, (st_c,)), (1, ng, (h_p, h_s))):
        each(first, last, lambda k: [f(k).wait_send() for f in fns])


def local(nsp, ntp, q1, q2, k1, k2, vals, lam, hg, stream, ow, g1, up, dn, g2):
    tok = q1.shape[0]
    heads = lam.shape[0]
    hv = vals.shape[1]
    vd = hv // heads
    d = ow.shape[1]
    nz, nth = nsp // 2, ntp // 2
    ng = 2 * nth
    share = tok // ntp
    fh = up.shape[1] // 2
    qk = q1.shape[1] // heads
    half, out_w = ng * share, dn.shape[1]
    pieces = 2 if out_w % 256 == 0 else 1
    units, pw = nz * pieces, out_w // pieces
    vm = pl.BlockSpec(memory_space=pltpu.VMEM)
    sm = pl.BlockSpec(memory_space=pltpu.SMEM)
    hbm = pl.BlockSpec(memory_space=pl.ANY)
    sem = lambda n: pltpu.SemaphoreType.DMA((2, n))
    return pl.pallas_call(
        functools.partial(kernel, nsp, ntp, heads, pieces),
        out_shape=jax.ShapeDtypeStruct((share, d), BF16),
        in_specs=[sm] + [hbm] * 12,
        out_specs=vm,
        scratch_shapes=[
            pltpu.VMEM((2, heads, 1, 128), F32),
            pltpu.VMEM((2, tok, heads * qk), BF16),
            pltpu.VMEM((2, tok, heads * qk), BF16),
            pltpu.VMEM((heads, tok, 2 * qk), BF16),
            pltpu.VMEM((heads, tok, 2 * qk + vd), BF16),
            pltpu.VMEM((1, vd), F32),
            pltpu.VMEM((1, d), F32),
            pltpu.VMEM((1, d), F32),
            pltpu.VMEM((2, tok, 2 * qk), BF16),
            pltpu.VMEM((2, 2 * tok, 2 * qk), BF16),
            pltpu.VMEM((2, 1, 2 * tok), F32),
            pltpu.VMEM((2, 1, 2 * tok), F32),
            pltpu.VMEM((2, vd, 2 * tok), F32),
            pltpu.VMEM((nsp, tok, 2 * qk + vd), BF16),
            pltpu.VMEM((nsp, up.shape[0], fh), BF16),
            pltpu.VMEM((nsp, fh, out_w), BF16),
            pltpu.VMEM((ntp,) + ow.shape, BF16),
            pltpu.VMEM((ntp, share, stream.shape[1]), BF16),
            pltpu.VMEM((2 * tok, vd), BF16),
            pltpu.VMEM((ntp, share, hv), BF16),
            pltpu.VMEM((share, d), F32),
            pltpu.VMEM((share, d), BF16),
            pltpu.VMEM((2, ng, share, d), BF16),
            pltpu.VMEM((2, half, fh), BF16),
            pltpu.VMEM((units, 2, half, pw), BF16),
            pltpu.VMEM((units, 2, half, pw), BF16),
            pltpu.VMEM((units, 2, half, pw), F32),
            pltpu.VMEM((units, 2, share, pw), F32),
            pltpu.VMEM((units, ng, 2, share, pw), BF16),
            pltpu.VMEM((units, ng, 2, share, pw), BF16),
            pltpu.SemaphoreType.DMA((4 + heads + 7,)),
            sem(1), sem(max(heads, 2)), sem(max(nz // 2 * heads, nz)), sem(nz),
            sem(nz), sem(nz), sem(units), sem(units),
            sem(nth), sem(nth), sem(ntp), sem(2 * ntp), sem(ng), sem(ng), sem(units), sem(units * ng),
        ],
        compiler_params=pltpu.CompilerParams(
            collective_id=0, has_side_effects=True, vmem_limit_bytes=60 * 1024 * 1024
        ),
    )(
        lam.reshape(1, heads), q1, q2, k1, k2, vals, hg.reshape(1, vd), stream, ow,
        g1.reshape(1, d), up, dn, g2.reshape(1, d),
    )


def solution(mesh):
    in_specs = (
        P("sp", "tp"),
        P("sp", "tp"),
        P("sp", "tp"),
        P("sp", "tp"),
        P("sp", "tp"),
        P("tp"),
        P(),
        P("sp", "tp"),
        P("tp", None),
        P(),
        P("sp", "tp"),
        P("tp", "sp"),
        P(),
    )
    body = functools.partial(local, mesh.shape["sp"], mesh.shape["tp"])
    return jax.shard_map(
        body, mesh=mesh, in_specs=in_specs, out_specs=P(("sp", "tp"), None), check_vma=False
    )
```

time: 106 us -> 108 us (1.019)
  Pallas kernels: 104 us -> 106 us
    pallas_call x1, Pallas kernels: 104 us -> 106 us  [local(): pl.pallas_call(functools.partial(kernel, nsp, ntp, heads, pieces), out_sh...]
where the time goes in v2:
time: 108 us
  Pallas kernels  106 us (98%)
  local copies, waits for them, and re-layouts  1.67 us (2%)
    pallas_call x1, Pallas kernels, local(): pl.pallas_call(functools.partial(kernel, nsp, ntp, heads, pieces), out_sh...  106 us

profile of v2, /device:TPU:0, one launch (start us, length us, event | category | flops | bytes accessed | tf_op | source)
XLA Modules:
  0.0 107.6 jit_solution(13452629872560681930)
XLA Ops:
  0.0 105.9 %shard_map.127 = bf16[64,2048]{1,0:T(8,128)(2,1)} custom-call(f32[1,2]{1,0:T(1,128)} %bitcast.6, bf16[256,128]{1,0:T(8,128)(2,1)} %q1_ref.1, bf16[256,128]{1,0:T(8,128)(2,1)} %q2_ref.1, bf16[256,128]{1,0:T(8,128)(2,1)} %k1_ref.1, bf16[256,128]{1,0:T(8,128)(2,1)} %k2_ref.1, bf16[256,256]{1,0:T(8,128)(2,1)} %v_ref.1, f32[1,128]{1,0:T(1,128)} %bitcast.7, ...), custom_call_target="tpu_custom_call" | custom-call | tf_op jit(solution)/shard_map/pallas_call | solution.py:502
  106.0 1.7 %copy.15 = bf16[64,2048]{1,0:T(8,128)(2,1)} copy(bf16[64,2048]{1,0:T(8,128)(2,1)} %shard_map.127) | data formatting | bytes 524288

commit v3 on v2

--- a/solution.py
+++ b/solution.py
@@ -142,7 +142,9 @@
         return rc(ref, ref, upy, zz, y_sp, t)
 
     def cols_of(p):
-        return pl.ds(p * pw, pw)
+        if pieces == 1:
+            return pl.ds(0, pw)
+        return pl.ds(p * pw if isinstance(p, int) else pl.multiple_of(p * pw, pw), pw)
 
     def dn_z(zz, p):
         return rc(
@@ -194,16 +196,36 @@
     def grp_dev(g):
         return (zh * 2 + g // nth) * 2 + y, lax.rem(g, nth) * 2 + c
 
-    def h_p(k):
-        sp, tp = grp_dev(lax.rem(grp + k, ng))
-        return rc(h_own, h_buf.at[c, grp], hps, k, sp, tp)
-
-    def h_s0():
-        return rc(h_own, h_buf.at[c, grp], hss, 0, s, sib_t)
-
-    def h_s(k):
-        g = lax.rem(grp + ng - k, ng)
-        return rc(h_buf.at[c, g], h_buf.at[c, g], hss, k, s, sib_t)
+    def h_rows(side, g, n):
+        return h_buf.at[side, g, pl.ds(n * (share // 2), share // 2), :]
+
+    def own_rows(n):
+        return h_own.at[pl.ds(n * (share // 2), share // 2), :]
+
+    def h_z(n):
+        return rc(own_rows(n), h_rows(c, grp, n), hps, n, mate * 2 + y, t, grp * 2 + n)
+
+    def h_x(k, n):
+        dest = lax.rem(x + k, nth) * 2 + c
+        return rc(own_rows(n), h_rows(c, grp, n), hps, k * 2 + n, s, dest, grp * 2 + n)
+
+    def h_far(k, n):
+        g = (1 - zl) * nth + x
+        ref = h_rows(c, g, n)
+        return rc(ref, ref, hps, (nth + k) * 2 + n, s, lax.rem(x + k, nth) * 2 + c, g * 2 + n)
+
+    def h_in(zz, k, n):
+        g = zz * nth + lax.rem(x + nth - k, nth)
+        ref = h_rows(c, g, n)
+        return rc(ref, ref, hps, 0, y_sp, t, g * 2 + n)
+
+    def h_s0(n):
+        return rc(own_rows(n), h_rows(c, grp, n), hss, grp * 2 + n, s, sib_t)
+
+    def h_s(zz, k, n, side=0):
+        g = zz * nth + lax.rem(x + nth - k, nth)
+        ref = h_rows(jnp.where(side == 0, c, 1 - c), g, n)
+        return rc(ref, ref, hss, g * 2 + n, s, sib_t)
 
     def sib_c(n):
         return rc(sib_snd.at[n], sib_buf.at[n], sbs, n, s, sib_t)
@@ -219,6 +241,8 @@
 
     def shared(zz):
         return (zz > z) == (mate > z)
+
+    inner = jnp.logical_not(shared(other(1, 0))) if npair > 1 else z < 0
 
     def others(fn):
         for m in range(2):
@@ -250,10 +274,10 @@
         ld.wait()
     pl.semaphore_wait(barrier, 4 * ntp - 1 + 8 * (npair - 1))
 
-    kv_out(lambda cp: cp.start(), False)
     for j in range(heads):
         pl.when(jnp.logical_not(to_self(j)))(lambda: q_c(j).start())
     kv_out(lambda cp: cp.start(), True)
+    kv_out(lambda cp: cp.start(), False)
     for j in range(heads):
         @pl.when(to_self(j))
         def _():
@@ -264,17 +288,25 @@
     each(1, ntp, lambda k: st_c(k).start())
     each(1, nth, lambda k: ow_x(k).start())
     ow_s0().start()
-    others(lambda zz: up_z(zz).start())
+    def up_late():
+        each(1, npair, lambda q: up_z(other(q, 1)).start())
+
+    up_y0().start()
     up_z(mate).start()
-    up_y0().start()
+    each(1, npair, lambda q: up_z(other(q, 0)).start())
+    pl.when(inner)(lambda: up_late())
+    for p in range(pieces):
+        dn_y0(p).start()
+
+    def dn_mate(early):
+        @pl.when(inner == early)
+        def _():
+            for p in range(pieces):
+                dn_z(mate, p).start()
+
+    dn_mate(True)
     for ld in gain_loads + [st_load, ow_load, up_load, dn_load]:
         ld.start()
-
-    def dn_far(early):
-        for p in range(pieces):
-            others(lambda zz: pl.when(shared(zz) != early)(lambda: dn_z(zz, p).start()))
-
-    dn_far(True)
 
     m_run[...] = jnp.full(m_run.shape, -1e30, F32)
     l_run[...] = jnp.zeros(l_run.shape, F32)
@@ -342,6 +374,13 @@
         up_zin(zz).wait_recv()
         up_y(zz).start()
 
+    def near_fwd():
+        each(1, npair, lambda q: up_fwd(other(q, 0)))
+
+    def far_fwd():
+        each(1, npair, lambda q: up_fwd(other(q, 1)))
+
+    pl.when(jnp.logical_not(inner))(lambda: up_late())
     up_fwd(mate)
     for k in range(1, nth):
         ow_x(k).wait_recv()
@@ -357,6 +396,7 @@
     ow_s0().wait_recv()
     for k in range(1, nth):
         ow_s(k).wait_recv()
+    pl.when(inner)(lambda: near_fwd())
     for b in range(ntp):
         at = slice(b * cols, (b + 1) * cols)
         tot = pre[:, at]
@@ -364,25 +404,37 @@
             tot += jnp.dot(at_buf[tt], ow_buf[tt, :, at], preferred_element_type=F32)
         pre[:, at] = tot
     h_own[...] = layer_norm(pre[...], g1[...]).astype(BF16)
-    each(1, ng, lambda k: h_p(k).start())
-    h_s0().start()
-    dn_far(False)
+    for n in range(2):
+        h_z(n).start()
+        for k in range(1, nth):
+            h_x(k, n).start()
+        h_s0(n).start()
+    dn_mate(False)
     for p in range(pieces):
-        dn_z(mate, p).start()
-    for p in range(pieces):
-        dn_y0(p).start()
+        others(lambda zz: dn_z(zz, p).start())
     h_buf[c, grp] = h_own[...]
-    others(up_fwd)
-
-    def h_fwd(k):
-        h_p(k).wait_recv()
-        h_s(k).start()
-
-    each(1, ng, h_fwd)
+    pl.when(jnp.logical_not(inner))(lambda: near_fwd())
+    far_fwd()
+
+    for n in range(2):
+        h_in(1 - zl, 0, n).wait_recv()
+        for k in range(1, nth):
+            h_far(k, n).start()
+        h_s(1 - zl, 0, n).start()
+    for n in range(2):
+        for k in range(1, nth):
+            h_in(zl, k, n).wait_recv()
+            h_s(zl, k, n).start()
+    for n in range(2):
+        for k in range(1, nth):
+            h_in(1 - zl, k, n).wait_recv()
+            h_s(1 - zl, k, n).start()
     up_load.wait()
     each(0, nz, lambda zz: up_y(zz, 1).wait_recv())
-    h_s0().wait_recv()
-    each(1, ng, lambda k: h_s(k).wait_recv())
+    for side in range(2):
+        for k in range(nth):
+            for n in range(2):
+                h_s(side, k, n, 1).wait_recv()
 
     half = ng * share
     for side in range(2):
@@ -411,33 +463,34 @@
         rows = pl.ds(pl.multiple_of(grp * share, share), share)
         own_part[n] = part[n, :, rows, :] + sib_buf[n, :, rows, :].astype(F32)
 
-    def down(w, carry):
-        zz = unit(w * pieces)
-        before = unit(w * pieces - pieces)
-        for p in range(pieces):
+    def down(i, carry):
+        @pl.when((i >= pieces) & (i < nz * pieces))
+        def _():
+            zz, p = unit(i), lax.rem(i, pieces)
+            dn_zin(zz, p).wait_recv()
+            dn_y(zz, p).start()
+
+        @pl.when(i > 1)
+        def _():
+            finish(unit(i - 2) * pieces + lax.rem(i - 2, pieces))
+
+        @pl.when(i > 0)
+        def _():
+            zz, p = unit(i - 1), lax.rem(i - 1, pieces)
             n = zz * pieces + p
-
-            @pl.when(w > 0)
-            def _():
-                dn_zin(zz, p).wait_recv()
-                dn_y(zz, p).start()
-
             dn_y(zz, p, 1).wait_recv()
-            at = slice(p * pw, (p + 1) * pw)
+            at = cols_of(p)
             for yy in range(2):
                 res = jnp.dot(act[1 - c], dn_buf[zz * 2 + yy, :, at], preferred_element_type=F32)
                 sib_snd[n, yy] = res.astype(BF16)
             sib_c(n).start()
             for yy in range(2):
                 part[n, yy] = jnp.dot(act[c], dn_buf[zz * 2 + yy, :, at], preferred_element_type=F32)
-            if p > 0:
-                finish(n - 1)
-            else:
-                pl.when(w > 0)(lambda: finish(before * pieces + pieces - 1))
+
         return carry
 
-    lax.fori_loop(0, nz, down, 0)
-    finish(unit(nz * pieces - pieces) * pieces + pieces - 1)
+    lax.fori_loop(0, nz * pieces + 1, down, 0)
+    finish(unit(nz * pieces - 1) * pieces + pieces - 1)
 
     for zz in range(nz):
         for p in range(pieces):
@@ -475,9 +528,17 @@
     each(0, nz, lambda zz: kv_s(zz, c).wait_send())
     lam_c().wait_send()
     ow_s0().wait_send()
-    h_s0().wait_send()
+    for n in range(2):
+        h_z(n).wait_send()
+        h_s0(n).wait_send()
+        for k in range(1, nth):
+            h_x(k, n).wait_send()
+            h_far(k, n).wait_send()
+            h_s(zl, k, n).wait_send()
+        for k in range(nth):
+            h_s(1 - zl, k, n).wait_send()
     each(0, nz * pieces, lambda n: [sib_c(n).wait_send()] + [red_c(n, k).wait_send() for k in range(1, ng)])
-    for first, last, fns in ((1, nth, (ow_x, ow_s)), (1, ntp, (st_c,)), (1, ng, (h_p, h_s))):
+    for first, last, fns in ((1, nth, (ow_x, ow_s)), (1, ntp, (st_c,))):
         each(first, last, lambda k: [f(k).wait_send() for f in fns])
 
 
@@ -538,7 +599,7 @@
             pltpu.SemaphoreType.DMA((4 + heads + 7,)),
             sem(1), sem(max(heads, 2)), sem(max(nz // 2 * heads, nz)), sem(nz),
             sem(nz), sem(nz), sem(units), sem(units),
-            sem(nth), sem(nth), sem(ntp), sem(2 * ntp), sem(ng), sem(ng), sem(units), sem(units * ng),
+            sem(nth), sem(nth), sem(ntp), sem(2 * ntp), sem(2 * ng), sem(2 * ng), sem(units), sem(units * ng),
         ],
         compiler_params=pltpu.CompilerParams(
             collective_id=0, has_side_effects=True, vmem_limit_bytes=60 * 1024 * 1024

time: 108 us -> 87.7 us (0.81)
  Pallas kernels: 106 us -> 85.8 us
    pallas_call x1, Pallas kernels: 106 us -> 85.8 us  [local(): pl.pallas_call(functools.partial(kernel, nsp, ntp, heads, pieces), out_sh...]
where the time goes in v3:
time: 87.7 us; the launch traced here: 87.5 us
  Pallas kernels  85.8 us (98%)
  local copies, waits for them, and re-layouts  1.67 us (2%)
    pallas_call x1, Pallas kernels, local(): pl.pallas_call(functools.partial(kernel, nsp, ntp, heads, pieces), out_sh...  85.8 us

profile of v3, /device:TPU:0, one launch (start us, length us, event | category | flops | bytes accessed | tf_op | source)
XLA Modules:
  0.0 87.5 jit_solution(9420180923591651758)
XLA Ops:
  0.0 85.8 %shard_map.127 = bf16[64,2048]{1,0:T(8,128)(2,1)} custom-call(f32[1,2]{1,0:T(1,128)} %bitcast.6, bf16[256,128]{1,0:T(8,128)(2,1)} %q1_ref.1, bf16[256,128]{1,0:T(8,128)(2,1)} %q2_ref.1, bf16[256,128]{1,0:T(8,128)(2,1)} %k1_ref.1, bf16[256,128]{1,0:T(8,128)(2,1)} %k2_ref.1, bf16[256,256]{1,0:T(8,128)(2,1)} %v_ref.1, f32[1,128]{1,0:T(1,128)} %bitcast.7, ...), custom_call_target="tpu_custom_call" | custom-call | tf_op jit(solution)/shard_map/pallas_call | solution.py:563
  85.8 1.7 %copy.15 = bf16[64,2048]{1,0:T(8,128)(2,1)} copy(bf16[64,2048]{1,0:T(8,128)(2,1)} %shard_map.127) | data formatting | bytes 524288

commit v4 on v2

v4 whole, which is shorter than its diff:
```python
import functools

import jax
import jax.numpy as jnp
from jax import lax
from jax.experimental import pallas as pl
from jax.experimental.pallas import tpu as pltpu
from jax.sharding import PartitionSpec as P

MESH = pl.DeviceIdType.MESH
F32, BF16 = jnp.float32, jnp.bfloat16
ALPHA = 2.0**0.5
NT = (((1,), (1,)), ((), ()))
TN = (((0,), (0,)), ((), ()))
KINDS = 13
LAM, Q, KV, KVS, UP, DN, OW, ST, AT, HP, HS, SIB, RED = range(KINDS)


def layer_norm(value, gain):
    centre = jnp.mean(value, axis=-1, keepdims=True)
    spread = jnp.mean(jnp.square(value - centre), axis=-1, keepdims=True)
    return (value - centre) * lax.rsqrt(spread + 1e-05) * gain


def kernel(
    nsp, ntp, heads, pieces,
    lam_ref, q1_ref, q2_ref, k1_ref, k2_ref, v_ref, hg_ref, st_ref, ow_ref, g1_ref, up_ref, dn_ref, g2_ref,
    out_ref,
    lam_all, qin, kin, qsl, slab, hg, g1, g2,
    q_buf, qm, m_run, l_run, acc, kv_buf, up_buf, dn_buf, ow_buf, st_buf, at_snd, at_buf,
    pre, h_own, h_buf, act, sib_snd, sib_buf, part, own_part, red_snd, red_buf,
    loc_sem, snd, one, rq, rkv, rkvs, rup, rdz, rdy, rox, rh, rsib, rred,
):
    s, t = lax.axis_index("sp"), lax.axis_index("tp")
    nz, nth = nsp // 2, ntp // 2
    npair = nz // 2
    ng = 2 * nth
    z, y = s // 2, s % 2
    zh, zl = z // 2, z % 2
    mate = zh * 2 + 1 - zl
    x, c = t // 2, t % 2
    sib_t = x * 2 + (1 - c)
    y_sp = z * 2 + (1 - y)
    grp = zl * nth + x
    tok = q1_ref.shape[0]
    share = tok // ntp
    fh = up_ref.shape[1] // 2
    vd = acc.shape[1]
    qw = q_buf.shape[2]
    qk = qw // 2
    d = pre.shape[1]
    out_w = dn_buf.shape[2]
    pw = out_w // pieces
    head_t = x * 2 + zl

    def rc(src, dst, kind, arrive, sp, tp):
        return pltpu.make_async_remote_copy(
            src_ref=src, dst_ref=dst, send_sem=snd.at[kind], recv_sem=arrive,
            device_id={"sp": sp, "tp": tp}, device_id_type=MESH,
        )

    def arrived(ref, sem):
        rc(ref, ref, 0, sem, y_sp, t).wait_recv()

    def left(ref, kind):
        rc(ref, ref, kind, one.at[LAM], y_sp, t).wait_send()

    def each(lo, hi, body):
        if hi - lo <= 4:
            for k in range(lo, hi):
                body(k)
        else:
            lax.fori_loop(lo, hi, lambda k, carry: (body(k), carry)[1], 0)

    def lc(src, dst, i):
        return pltpu.make_async_copy(src, dst, loc_sem.at[i])

    def up_half(j):
        return up_ref.at[:, pl.ds(pl.multiple_of(j * fh, fh), fh)]

    def dn_rows(j):
        return pl.ds(pl.multiple_of(j * fh, fh), fh)

    def rows_of(tt):
        return pl.ds(pl.multiple_of(tt * share, share), share)

    qk_loads = [
        lc(q1_ref, qin.at[0], 0),
        lc(q2_ref, qin.at[1], 1),
        lc(k1_ref, kin.at[0], 2),
        lc(k2_ref, kin.at[1], 3),
    ]
    v_loads = [
        lc(v_ref.at[:, pl.ds(j * vd, vd)], slab.at[j, :, pl.ds(qw, vd)], 4 + j) for j in range(heads)
    ]
    n0 = 4 + heads
    gain_loads = [lc(hg_ref, hg, n0), lc(g1_ref, g1, n0 + 1), lc(g2_ref, g2, n0 + 2)]
    up_load = lc(up_half(zl), up_buf.at[s], n0 + 3)
    dn_load = lc(dn_ref.at[dn_rows(zl), :], dn_buf.at[s], n0 + 4)
    ow_load = lc(ow_ref, ow_buf.at[t], n0 + 5)
    st_load = lc(st_ref.at[rows_of(t), :], st_buf.at[t], n0 + 6)
    for ld in qk_loads + v_loads:
        ld.start()

    def lam_c():
        return rc(lam_all.at[c], lam_all.at[c], LAM, one.at[LAM], s, sib_t)

    def to_self(j):
        return (c == zl) & (y == c) & (j == y)

    self_worker = (c == zl) & (y == c)

    def q_c(j):
        return rc(qsl.at[j], q_buf.at[zl], Q, rq.at[zl], (zh * 2 + c) * 2 + j, x * 2 + y)

    def kv_c(r, j):
        return rc(slab.at[j], kv_buf.at[s], KV, rkv.at[z], (r * 2 + c) * 2 + j, x * 2 + y)

    def kv_s(zz):
        ref = kv_buf.at[zz * 2 + c]
        return rc(ref, ref, KVS, rkvs.at[zz], s, sib_t)

    def kv_out(fn, own):
        for j in range(heads):
            if own:
                pl.when(jnp.logical_not(to_self(j)))(lambda: fn(kv_c(zh, j)))
            else:
                each(1, npair, lambda q: fn(kv_c(lax.rem(zh + q, npair), j)))

    ur = up_ref.shape[0] // 2

    def up_rows(p):
        return pl.ds(p * ur, ur)

    def up_part(j, p):
        return up_ref.at[up_rows(p), pl.ds(pl.multiple_of(j * fh, fh), fh)]

    def up_z(zz, p):
        return rc(up_part(zz % 2, p), up_buf.at[s, up_rows(p)], UP, rup.at[z * 2 + p], zz * 2 + y, t)

    def up_y0(p):
        return rc(up_part(zl, p), up_buf.at[s, up_rows(p)], UP, one.at[UP], y_sp, t)

    def up_fwd(zz, p):
        ref = up_buf.at[zz * 2 + y, up_rows(p)]
        arrived(ref, rup.at[zz * 2 + p])
        rc(ref, ref, UP, one.at[UP], y_sp, t).start()

    def cols_of(p):
        if pieces == 1:
            return pl.ds(0, pw)
        return pl.ds(p * pw if isinstance(p, int) else pl.multiple_of(p * pw, pw), pw)

    def dn_part(j, p):
        return dn_ref.at[dn_rows(j), cols_of(p)]

    def dn_z(zz, p):
        return rc(
            dn_part(zz % 2, p), dn_buf.at[s, :, cols_of(p)], DN, rdz.at[z * pieces + p], zz * 2 + y, t
        )

    def dn_y0(p):
        return rc(dn_part(zl, p), dn_buf.at[s, :, cols_of(p)], DN, rdy.at[z * pieces + p], y_sp, t)

    def dn_fwd(zz, p):
        ref = dn_buf.at[zz * 2 + y, :, cols_of(p)]
        arrived(ref, rdz.at[zz * pieces + p])
        rc(ref, ref, DN, rdy.at[zz * pieces + p], y_sp, t).start()

    def ow_x(k):
        return rc(ow_ref, ow_buf.at[t], OW, rox.at[k], s, lax.rem(x + k, nth) * 2 + c)

    def ow_s0():
        return rc(ow_ref, ow_buf.at[t], OW, one.at[OW], s, sib_t)

    def ow_fwd(k):
        ref = ow_buf.at[lax.rem(x + nth - k, nth) * 2 + c]
        arrived(ref, rox.at[k])
        rc(ref, ref, OW, one.at[OW], s, sib_t).start()

    def st_c(k):
        td = lax.rem(t + k, ntp)
        return rc(st_ref.at[rows_of(td), :], st_buf.at[t], ST, one.at[ST], s, td)

    def at_cols():
        return pl.ds(pl.multiple_of(y * vd, vd), vd)

    def at_c(i, tt):
        rows = pl.ds((i * ntp + tt) * share, share)
        return rc(
            at_snd.at[rows, :], at_buf.at[head_t, :, at_cols()], AT, one.at[AT], (zh * 2 + i) * 2 + c, tt
        )

    def at_all(fn):
        pl.when(y == c)(lambda: fn(at_snd.at[pl.ds(0, 2 * tok - share)]))
        pl.when(y != c)(lambda: fn(at_snd.at[pl.ds(0, 2 * tok)]))

    def grp_dev(g):
        return (zh * 2 + g // nth) * 2 + y, lax.rem(g, nth) * 2 + c

    def h_rows(g, n):
        return h_buf.at[c, g, pl.ds(n * (share // 2), share // 2), :]

    def own_rows(n):
        return h_own.at[pl.ds(n * (share // 2), share // 2), :]

    def h_z(n):
        return rc(own_rows(n), h_rows(grp, n), HP, rh.at[grp * 2 + n], mate * 2 + y, t)

    def h_x(k, n):
        dest = lax.rem(x + k, nth) * 2 + c
        return rc(own_rows(n), h_rows(grp, n), HP, rh.at[grp * 2 + n], s, dest)

    def h_s0(n):
        return rc(own_rows(n), h_rows(grp, n), HS, one.at[HS], s, sib_t)

    def h_fwd(zz, k, n, far=False):
        g = zz * nth + lax.rem(x + nth - k, nth)
        ref = h_rows(g, n)
        arrived(ref, rh.at[g * 2 + n])
        if far:
            for i in range(1, nth):
                rc(ref, ref, HP, rh.at[g * 2 + n], s, lax.rem(x + i, nth) * 2 + c).start()
        rc(ref, ref, HS, one.at[HS], s, sib_t).start()

    def sib_c(n):
        return rc(sib_snd.at[n], sib_buf.at[n], SIB, rsib.at[n], s, sib_t)

    def red_c(n, k):
        g = lax.rem(grp + k, ng)
        sp, tp = grp_dev(g)
        return rc(red_snd.at[n, g], red_buf.at[n, grp], RED, rred.at[n], sp, tp)

    def other(q, m):
        r = lax.rem(zh + q, npair)
        return r * 2 + jnp.where(r > zh, m, 1 - m)

    def shared(zz):
        return (zz > z) == (mate > z)

    inner = jnp.logical_not(shared(other(1, 0))) if npair > 1 else z < 0

    def others(fn):
        for m in range(2):
            each(1, npair, lambda q: fn(other(q, m)))

    barrier = pltpu.get_barrier_semaphore()

    def greet(sp, tp):
        pl.semaphore_signal(barrier, inc=1, device_id={"sp": sp, "tp": tp}, device_id_type=MESH)

    for o in range(4 * ntp):
        sp, tt = zh * 4 + o // ntp, o % ntp
        pl.when((sp != s) | (tt != t))(functools.partial(greet, sp, tt))

    def greet_far(q):
        for o in range(8):
            greet(lax.rem(zh + q, npair) * 4 + o // 2, x * 2 + o % 2)

    each(1, npair, greet_far)

    for ld in qk_loads:
        ld.wait()
    for j in range(heads):
        at = slice(j * qk, (j + 1) * qk)
        qsl[j] = jnp.concatenate([qin[0, :, at], qin[1, :, at]], axis=1)
        slab[j, :, :qw] = jnp.concatenate([kin[0, :, at], kin[1, :, at]], axis=1)
        lam_all[c, j] = jnp.full(lam_all.shape[2:], lam_ref[0, j], F32)
    for ld in v_loads:
        ld.wait()
    pl.semaphore_wait(barrier, 4 * ntp - 1 + 8 * (npair - 1))

    for j in range(heads):
        pl.when(jnp.logical_not(to_self(j)))(lambda: q_c(j).start())
    kv_out(lambda cp: cp.start(), True)
    kv_out(lambda cp: cp.start(), False)
    for j in range(heads):
        @pl.when(to_self(j))
        def _():
            q_buf[zl] = qsl[j]
            kv_buf[s] = slab[j]

    lam_c().start()
    each(1, nth, lambda k: ow_x(k).start())
    each(1, ntp, lambda k: st_c(k).start())
    ow_s0().start()
    def up_far(p):
        each(1, npair, lambda q: up_z(other(q, 1), p).start())
        each(1, npair, lambda q: up_z(other(q, 0), p).start())

    for p in range(2):
        up_y0(p).start()
    for p in range(2):
        up_z(mate, p).start()
    up_far(0)
    pl.when(inner)(lambda: up_far(1))
    for p in range(pieces):
        dn_y0(p).start()
    for ld in gain_loads + [st_load, ow_load, up_load, dn_load]:
        ld.start()

    m_run[...] = jnp.full(m_run.shape, -1e30, F32)
    l_run[...] = jnp.zeros(l_run.shape, F32)
    acc[...] = jnp.zeros(acc.shape, F32)
    scale = qk ** (-0.5)
    lane = lax.broadcasted_iota(jnp.int32, (tok, qw), 1)
    for i in range(2):
        pl.when(jnp.logical_not(self_worker & (zl == i)))(lambda: arrived(q_buf.at[i], rq.at[i]))
        qv = q_buf[i].astype(F32) * scale
        for mp in range(2):
            keep = (lane >= mp * qk) & (lane < (mp + 1) * qk)
            qm[mp, i * tok : (i + 1) * tok, :] = jnp.where(keep, qv, 0.0).astype(BF16)

    def absorb(block):
        v = block[:, qw:]
        for r in range(2):
            sc = lax.dot_general(block[:, :qw], qm[r], NT, preferred_element_type=F32)
            old = m_run[r]
            new = jnp.maximum(old, jnp.max(sc, axis=0, keepdims=True))
            fac = jnp.exp(old - new)
            ex = jnp.exp(sc - new)
            l_run[r] = l_run[r] * fac + jnp.sum(ex, axis=0, keepdims=True)
            acc[r] = acc[r] * fac + lax.dot_general(
                v, ex.astype(BF16), TN, preferred_element_type=F32
            )
            m_run[r] = new

    def step(i, carry):
        zz = lax.rem(zh * 2 + i // 2, nz)
        own = lax.rem(i, 2) == 0

        @pl.when(own)
        def _():
            direct = kv_buf.at[zz * 2 + c]
            pl.when(jnp.logical_not(self_worker & (zz == z)))(lambda: arrived(direct, rkv.at[zz]))
            kv_s(zz).start()

        pl.when(jnp.logical_not(own))(lambda: arrived(kv_buf.at[zz * 2 + 1 - c], rkvs.at[zz]))
        absorb(kv_buf.at[zz * 2 + jnp.where(own, c, 1 - c)])
        return carry

    lax.fori_loop(0, nsp, step, 0)

    for ld in gain_loads:
        ld.wait()
    arrived(lam_all.at[c], one.at[LAM])
    lam = lam_all[zl, y][:, :1]
    mixed = acc[0] / l_run[0] - lam * (acc[1] / l_run[1])
    inv = lax.rsqrt(jnp.mean(jnp.square(mixed), axis=0, keepdims=True) + 1e-05)
    normed = jnp.transpose(mixed * inv) * hg[...] * 0.8
    at_snd[...] = normed.astype(BF16)
    spots = [(i, tt) for i in range(2) for tt in range(ntp)]

    def at_mine(i, tt):
        return (i == zl) & (y == c) & (tt == t)

    for i, tt in spots:
        pl.when(jnp.logical_not(at_mine(i, tt)))(lambda: at_c(i, tt).start())

        @pl.when(at_mine(i, tt))
        def _():
            n = (i * ntp + tt) * share
            at_buf[head_t, :, at_cols()] = at_snd[n : n + share, :]

    def others_fwd(p):
        each(1, npair, lambda q: [up_fwd(other(q, m), p) for m in range(2)])

    pl.when(jnp.logical_not(inner))(lambda: up_far(1))
    for p in range(2):
        up_fwd(mate, p)
    for k in range(1, nth):
        ow_fwd(k)
    others_fwd(0)
    st_load.wait()
    arrived(st_buf.at[pl.ds(0, ntp - 1)], one.at[ST])
    cols = st_ref.shape[1]
    for b in range(ntp):
        pre[:, b * cols : (b + 1) * cols] = ALPHA * st_buf[b].astype(F32)
    at_all(lambda ref: arrived(ref, one.at[AT]))
    ow_load.wait()
    arrived(ow_buf.at[pl.ds(0, nth)], one.at[OW])
    for b in range(ntp):
        at = slice(b * cols, (b + 1) * cols)
        tot = pre[:, at]
        for tt in range(ntp):
            tot += jnp.dot(at_buf[tt], ow_buf[tt, :, at], preferred_element_type=F32)
        pre[:, at] = tot
    h_own[...] = layer_norm(pre[...], g1[...]).astype(BF16)
    for n in range(2):
        h_z(n).start()
        for k in range(1, nth):
            h_x(k, n).start()
        h_s0(n).start()
    for p in range(pieces):
        dn_z(mate, p).start()
    for p in range(pieces):
        each(1, npair, lambda q: dn_z(other(q, 0), p).start())
    h_buf[c, grp] = h_own[...]
    others_fwd(1)

    for n in range(2):
        h_fwd(1 - zl, 0, n, True)
    for p in range(pieces):
        each(1, npair, lambda q: dn_z(other(q, 1), p).start())
    for zz in (zl, 1 - zl):
        for n in range(2):
            for k in range(1, nth):
                h_fwd(zz, k, n)
    up_load.wait()
    arrived(up_buf.at[pl.ds(0, nz)], one.at[UP])
    arrived(h_buf.at[0], one.at[HS])

    half = ng * share
    for side in range(2):
        parts = 2 if fh % 256 == 0 else 1
        for n in range(parts):
            wide = fh // parts
            at = slice(n * wide, (n + 1) * wide)
            hid = h_buf[side].reshape(half, d)
            w = up_buf[:, :, at].reshape(d, wide)
            up = jnp.dot(hid, w, preferred_element_type=F32)
            act[side, :, at] = jnp.square(jnp.maximum(up, 0.0)).astype(BF16)
    dn_load.wait()

    steps = nz * pieces

    def unit(i):
        r = lax.rem(i, 2 * pieces)
        far = other(i // (2 * pieces), lax.rem(r, 2))
        zz = jnp.where(i < pieces, z, jnp.where(i < 2 * pieces, mate, far))
        return zz, jnp.where(i < 2 * pieces, lax.rem(i, pieces), r // 2)

    def index(i):
        zz, p = unit(i)
        return zz * pieces + p

    def finish(n):
        arrived(sib_buf.at[n], rsib.at[n])
        for k in range(ng - 1, 0, -1):
            g = lax.rem(grp + k, ng)
            rows = pl.ds(pl.multiple_of(g * share, share), share)
            red_snd[n, g] = (part[n, :, rows, :] + sib_buf[n, :, rows, :].astype(F32)).astype(BF16)
            red_c(n, k).start()
        rows = pl.ds(pl.multiple_of(grp * share, share), share)
        own_part[n] = part[n, :, rows, :] + sib_buf[n, :, rows, :].astype(F32)

    ahead, lead = pieces, 2

    def down(i, carry):
        pl.when((i + lead >= ahead) & (i + lead < steps))(lambda: dn_fwd(*unit(i + lead)))
        pl.when(i > 0)(lambda: finish(index(i - 1)))
        zz, p = unit(i)
        n = zz * pieces + p
        arrived(dn_buf.at[zz * 2 + 1 - y, :, cols_of(p)], rdy.at[n])
        at = cols_of(p)
        for yy in range(2):
            res = jnp.dot(act[1 - c], dn_buf[zz * 2 + yy, :, at], preferred_element_type=F32)
            sib_snd[n, yy] = res.astype(BF16)
        sib_c(n).start()
        for yy in range(2):
            part[n, yy] = jnp.dot(act[c], dn_buf[zz * 2 + yy, :, at], preferred_element_type=F32)
        return carry

    lax.fori_loop(0, steps, down, 0)
    finish(index(steps - 1))

    for zz in range(nz):
        for p in range(pieces):
            n = zz * pieces + p
            arrived(red_buf.at[n, pl.ds(0, ng - 1)], rred.at[n])
            for yy in range(2):
                lo = (zz * 2 + yy) * out_w + p * pw
                at = slice(lo, lo + pw)
                tot = own_part[n, yy] + ALPHA * h_own[:, at].astype(F32)
                for k in range(ng - 1, 0, -1):
                    tot += red_buf[n, lax.rem(grp + ng - k, ng), yy].astype(F32)
                pre[:, at] = tot
    out_ref[...] = layer_norm(pre[...], g2[...]).astype(BF16)

    for kind, buf, most in ((Q, qsl, heads), (KV, kv_buf, npair * heads)):
        pl.when(self_worker)(lambda: left(buf.at[pl.ds(0, most - 1)], kind))
        pl.when(jnp.logical_not(self_worker))(lambda: left(buf.at[pl.ds(0, most)], kind))
    at_all(lambda ref: left(ref, AT))
    left(lam_all.at[c], LAM)
    left(kv_buf.at[pl.ds(0, nz)], KVS)
    left(up_buf.at[pl.ds(0, nsp - 1)], UP)
    left(dn_buf.at[pl.ds(0, nsp - 1)], DN)
    left(ow_buf.at[pl.ds(0, ntp - 1)], OW)
    left(st_buf.at[pl.ds(0, ntp - 1)], ST)
    left(h_buf.at[0, pl.ds(0, ng - 1)], HP)
    left(h_buf.at[0], HS)
    left(sib_snd, SIB)
    left(red_snd.at[:, pl.ds(0, ng - 1)], RED)


def local(nsp, ntp, q1, q2, k1, k2, vals, lam, hg, stream, ow, g1, up, dn, g2):
    tok = q1.shape[0]
    heads = lam.shape[0]
    hv = vals.shape[1]
    vd = hv // heads
    d = ow.shape[1]
    nz, nth = nsp // 2, ntp // 2
    ng = 2 * nth
    share = tok // ntp
    fh = up.shape[1] // 2
    qk = q1.shape[1] // heads
    half, out_w = ng * share, dn.shape[1]
    pieces = 2 if out_w % 256 == 0 else 1
    units, pw = nz * pieces, out_w // pieces
    vm = pl.BlockSpec(memory_space=pltpu.VMEM)
    sm = pl.BlockSpec(memory_space=pltpu.SMEM)
    hbm = pl.BlockSpec(memory_space=pl.ANY)
    sems = (KINDS, KINDS, 2, nz, nz, 2 * nz, units, units, nth, 2 * ng, units, units)
    return pl.pallas_call(
        functools.partial(kernel, nsp, ntp, heads, pieces),
        out_shape=pltpu.VMEM((share, d), BF16),
        in_specs=[sm] + [hbm] * 12,
        out_specs=vm,
        scratch_shapes=[
            pltpu.VMEM((2, heads, 1, 128), F32),
            pltpu.VMEM((2, tok, heads * qk), BF16),
            pltpu.VMEM((2, tok, heads * qk), BF16),
            pltpu.VMEM((heads, tok, 2 * qk), BF16),
            pltpu.VMEM((heads, tok, 2 * qk + vd), BF16),
            pltpu.VMEM((1, vd), F32),
            pltpu.VMEM((1, d), F32),
            pltpu.VMEM((1, d), F32),
            pltpu.VMEM((2, tok, 2 * qk), BF16),
            pltpu.VMEM((2, 2 * tok, 2 * qk), BF16),
            pltpu.VMEM((2, 1, 2 * tok), F32),
            pltpu.VMEM((2, 1, 2 * tok), F32),
            pltpu.VMEM((2, vd, 2 * tok), F32),
            pltpu.VMEM((nsp, tok, 2 * qk + vd), BF16),
            pltpu.VMEM((nsp, up.shape[0], fh), BF16),
            pltpu.VMEM((nsp, fh, out_w), BF16),
            pltpu.VMEM((ntp,) + ow.shape, BF16),
            pltpu.VMEM((ntp, share, stream.shape[1]), BF16),
            pltpu.VMEM((2 * tok, vd), BF16),
            pltpu.VMEM((ntp, share, hv), BF16),
            pltpu.VMEM((share, d), F32),
            pltpu.VMEM((share, d), BF16),
            pltpu.VMEM((2, ng, share, d), BF16),
            pltpu.VMEM((2, half, fh), BF16),
            pltpu.VMEM((units, 2, half, pw), BF16),
            pltpu.VMEM((units, 2, half, pw), BF16),
            pltpu.VMEM((units, 2, half, pw), F32),
            pltpu.VMEM((units, 2, share, pw), F32),
            pltpu.VMEM((units, ng, 2, share, pw), BF16),
            pltpu.VMEM((units, ng, 2, share, pw), BF16),
            pltpu.SemaphoreType.DMA((4 + heads + 7,)),
            *[pltpu.SemaphoreType.DMA((n,)) for n in sems],
        ],
        compiler_params=pltpu.CompilerParams(
            collective_id=0, has_side_effects=True, vmem_limit_bytes=60 * 1024 * 1024
        ),
    )(
        lam.reshape(1, heads), q1, q2, k1, k2, vals, hg.reshape(1, vd), stream, ow,
        g1.reshape(1, d), up, dn, g2.reshape(1, d),
    )


def solution(mesh):
    in_specs = (
        P("sp", "tp"),
        P("sp", "tp"),
        P("sp", "tp"),
        P("sp", "tp"),
        P("sp", "tp"),
        P("tp"),
        P(),
        P("sp", "tp"),
        P("tp", None),
        P(),
        P("sp", "tp"),
        P("tp", "sp"),
        P(),
    )
    body = functools.partial(local, mesh.shape["sp"], mesh.shape["tp"])
    return jax.shard_map(
        body, mesh=mesh, in_specs=in_specs, out_specs=P(("sp", "tp"), None), check_vma=False
    )
```

time: 108 us -> 79.2 us (0.73)
  Pallas kernels: 106 us -> 78.3 us
    pallas_call x1, Pallas kernels: 106 us -> 78.3 us  [local(): pl.pallas_call(functools.partial(kernel, nsp, ntp, heads, pieces), out_sh...]
where the time goes in v4:
time: 79.2 us; the launch traced here: 79 us
  Pallas kernels  78.3 us (99%)
    pallas_call x1, Pallas kernels, local(): pl.pallas_call(functools.partial(kernel, nsp, ntp, heads, pieces), out_sh...  78.3 us

profile of v4, /device:TPU:0, one launch (start us, length us, event | category | flops | bytes accessed | tf_op | source)
XLA Modules:
  0.0 79.0 jit_solution(10537567668334405960)
XLA Ops:
  0.0 78.3 %shard_map.127 = bf16[64,2048]{1,0:T(8,128)(2,1)S(1)} custom-call(f32[1,2]{1,0:T(1,128)} %bitcast.6, bf16[256,128]{1,0:T(8,128)(2,1)} %q1_ref.1, bf16[256,128]{1,0:T(8,128)(2,1)} %q2_ref.1, bf16[256,128]{1,0:T(8,128)(2,1)} %k1_ref.1, bf16[256,128]{1,0:T(8,128)(2,1)} %k2_ref.1, bf16[256,256]{1,0:T(8,128)(2,1)} %v_ref.1, f32[1,128]{1,0:T(1,128)} %bitcast.7, ...), custom_call_target="tpu_custom_call" | custom-call | tf_op jit(solution)/shard_map/pallas_call | solution.py:514
  78.3 0.7 copy.15

commit v5 on v4

--- a/solution.py
+++ b/solution.py
@@ -26,7 +26,7 @@
     nsp, ntp, heads, pieces,
     lam_ref, q1_ref, q2_ref, k1_ref, k2_ref, v_ref, hg_ref, st_ref, ow_ref, g1_ref, up_ref, dn_ref, g2_ref,
     out_ref,
-    lam_all, qin, kin, qsl, slab, hg, g1, g2,
+    lam_in, lam_all, qin, kin, qsl, slab, hg, g1, g2,
     q_buf, qm, m_run, l_run, acc, kv_buf, up_buf, dn_buf, ow_buf, st_buf, at_snd, at_buf,
     pre, h_own, h_buf, act, sib_snd, sib_buf, part, own_part, red_snd, red_buf,
     loc_sem, snd, one, rq, rkv, rkvs, rup, rdz, rdy, rox, rh, rsib, rred,
@@ -93,14 +93,13 @@
     v_loads = [
         lc(v_ref.at[:, pl.ds(j * vd, vd)], slab.at[j, :, pl.ds(qw, vd)], 4 + j) for j in range(heads)
     ]
-    n0 = 4 + heads
+    n0 = 5 + heads
+    lam_load = lc(lam_ref, lam_in, 4 + heads)
     gain_loads = [lc(hg_ref, hg, n0), lc(g1_ref, g1, n0 + 1), lc(g2_ref, g2, n0 + 2)]
     up_load = lc(up_half(zl), up_buf.at[s], n0 + 3)
     dn_load = lc(dn_ref.at[dn_rows(zl), :], dn_buf.at[s], n0 + 4)
     ow_load = lc(ow_ref, ow_buf.at[t], n0 + 5)
     st_load = lc(st_ref.at[rows_of(t), :], st_buf.at[t], n0 + 6)
-    for ld in qk_loads + v_loads:
-        ld.start()
 
     def lam_c():
         return rc(lam_all.at[c], lam_all.at[c], LAM, one.at[LAM], s, sib_t)
@@ -258,14 +257,16 @@
             greet(lax.rem(zh + q, npair) * 4 + o // 2, x * 2 + o % 2)
 
     each(1, npair, greet_far)
-
-    for ld in qk_loads:
+    for ld in qk_loads + v_loads + [lam_load]:
+        ld.start()
+
+    for ld in qk_loads + [lam_load]:
         ld.wait()
     for j in range(heads):
         at = slice(j * qk, (j + 1) * qk)
         qsl[j] = jnp.concatenate([qin[0, :, at], qin[1, :, at]], axis=1)
         slab[j, :, :qw] = jnp.concatenate([kin[0, :, at], kin[1, :, at]], axis=1)
-        lam_all[c, j] = jnp.full(lam_all.shape[2:], lam_ref[0, j], F32)
+        lam_all[c, j] = jnp.full(lam_all.shape[2:], lam_in[0, j], F32)
     for ld in v_loads:
         ld.wait()
     pl.semaphore_wait(barrier, 4 * ntp - 1 + 8 * (npair - 1))
@@ -508,15 +509,15 @@
     pieces = 2 if out_w % 256 == 0 else 1
     units, pw = nz * pieces, out_w // pieces
     vm = pl.BlockSpec(memory_space=pltpu.VMEM)
-    sm = pl.BlockSpec(memory_space=pltpu.SMEM)
     hbm = pl.BlockSpec(memory_space=pl.ANY)
     sems = (KINDS, KINDS, 2, nz, nz, 2 * nz, units, units, nth, 2 * ng, units, units)
     return pl.pallas_call(
         functools.partial(kernel, nsp, ntp, heads, pieces),
         out_shape=pltpu.VMEM((share, d), BF16),
-        in_specs=[sm] + [hbm] * 12,
+        in_specs=[hbm] * 13,
         out_specs=vm,
         scratch_shapes=[
+            pltpu.SMEM((1, heads), F32),
             pltpu.VMEM((2, heads, 1, 128), F32),
             pltpu.VMEM((2, tok, heads * qk), BF16),
             pltpu.VMEM((2, tok, heads * qk), BF16),
@@ -547,7 +548,7 @@
             pltpu.VMEM((units, 2, share, pw), F32),
             pltpu.VMEM((units, ng, 2, share, pw), BF16),
             pltpu.VMEM((units, ng, 2, share, pw), BF16),
-            pltpu.SemaphoreType.DMA((4 + heads + 7,)),
+            pltpu.SemaphoreType.DMA((5 + heads + 7,)),
             *[pltpu.SemaphoreType.DMA((n,)) for n in sems],
         ],
         compiler_params=pltpu.CompilerParams(

time: 79.2 us -> 78.6 us (level)
  no operation moved by 1% of the time
where the time goes in v5:
time: 78.6 us; the launch traced here: 78.4 us
  Pallas kernels  77.7 us (99%)
    pallas_call x1, Pallas kernels, local(): pl.pallas_call(functools.partial(kernel, nsp, ntp, heads, pieces), out_sh...  77.7 us

profile of v5, /device:TPU:0, one launch (start us, length us, event | category | flops | bytes accessed | tf_op | source)
XLA Modules:
  0.0 78.4 jit_solution(13973576727733807327)
XLA Ops:
  0.0 77.7 %shard_map.127 = bf16[64,2048]{1,0:T(8,128)(2,1)S(1)} custom-call(f32[1,2]{1,0:T(1,128)} %bitcast.6, bf16[256,128]{1,0:T(8,128)(2,1)} %q1_ref.1, bf16[256,128]{1,0:T(8,128)(2,1)} %q2_ref.1, bf16[256,128]{1,0:T(8,128)(2,1)} %k1_ref.1, bf16[256,128]{1,0:T(8,128)(2,1)} %k2_ref.1, bf16[256,256]{1,0:T(8,128)(2,1)} %v_ref.1, f32[1,128]{1,0:T(1,128)} %bitcast.7, ...), custom_call_target="tpu_custom_call" | custom-call | tf_op jit(solution)/shard_map/pallas_call | solution.py:514
  77.7 0.7 copy.15

commit v6 on v5

--- a/solution.py
+++ b/solution.py
@@ -13,7 +13,8 @@
 NT = (((1,), (1,)), ((), ()))
 TN = (((0,), (0,)), ((), ()))
 KINDS = 13
-LAM, Q, KV, KVS, UP, DN, OW, ST, AT, HP, HS, SIB, RED = range(KINDS)
+SHARED = 6
+LAM, UP, OW, ST, AT, HS, Q, KV, KVS, DN, HP, SIB, RED = range(KINDS)
 
 
 def layer_norm(value, gain):
@@ -221,9 +222,6 @@
             for i in range(1, nth):
                 rc(ref, ref, HP, rh.at[g * 2 + n], s, lax.rem(x + i, nth) * 2 + c).start()
         rc(ref, ref, HS, one.at[HS], s, sib_t).start()
-
-    def sib_c(n):
-        return rc(sib_snd.at[n], sib_buf.at[n], SIB, rsib.at[n], s, sib_t)
 
     def red_c(n, k):
         g = lax.rem(grp + k, ng)
@@ -454,12 +452,14 @@
         n = zz * pieces + p
         arrived(dn_buf.at[zz * 2 + 1 - y, :, cols_of(p)], rdy.at[n])
         at = cols_of(p)
+        w = jnp.concatenate([dn_buf[zz * 2, :, at], dn_buf[zz * 2 + 1, :, at]], axis=1)
+        res = jnp.dot(act[1 - c], w, preferred_element_type=F32)
         for yy in range(2):
-            res = jnp.dot(act[1 - c], dn_buf[zz * 2 + yy, :, at], preferred_element_type=F32)
-            sib_snd[n, yy] = res.astype(BF16)
-        sib_c(n).start()
+            sib_snd[n, yy] = res[:, yy * pw : (yy + 1) * pw].astype(BF16)
+            rc(sib_snd.at[n, yy], sib_buf.at[n, yy], SIB, rsib.at[n], s, sib_t).start()
+        res = jnp.dot(act[c], w, preferred_element_type=F32)
         for yy in range(2):
-            part[n, yy] = jnp.dot(act[c], dn_buf[zz * 2 + yy, :, at], preferred_element_type=F32)
+            part[n, yy] = res[:, yy * pw : (yy + 1) * pw]
         return carry
 
     lax.fori_loop(0, steps, down, 0)
@@ -510,7 +510,7 @@
     units, pw = nz * pieces, out_w // pieces
     vm = pl.BlockSpec(memory_space=pltpu.VMEM)
     hbm = pl.BlockSpec(memory_space=pl.ANY)
-    sems = (KINDS, KINDS, 2, nz, nz, 2 * nz, units, units, nth, 2 * ng, units, units)
+    sems = (KINDS, SHARED, 2, nz, nz, 2 * nz, units, units, nth, 2 * ng, units, units)
     return pl.pallas_call(
         functools.partial(kernel, nsp, ntp, heads, pieces),
         out_shape=pltpu.VMEM((share, d), BF16),

time: 78.6 us -> 78.5 us (level)
  no operation moved by 1% of the time
where the time goes in v6:
time: 78.5 us; the launch traced here: 78.4 us
  Pallas kernels  77.7 us (99%)
    pallas_call x1, Pallas kernels, local(): pl.pallas_call(functools.partial(kernel, nsp, ntp, heads, pieces), out_sh...  77.7 us

profile of v6, /device:TPU:0, one launch (start us, length us, event | category | flops | bytes accessed | tf_op | source)
XLA Modules:
  0.0 78.4 jit_solution(5125516999270915441)
XLA Ops:
  0.0 77.7 %shard_map.127 = bf16[64,2048]{1,0:T(8,128)(2,1)S(1)} custom-call(f32[1,2]{1,0:T(1,128)} %bitcast.6, bf16[256,128]{1,0:T(8,128)(2,1)} %q1_ref.1, bf16[256,128]{1,0:T(8,128)(2,1)} %q2_ref.1, bf16[256,128]{1,0:T(8,128)(2,1)} %k1_ref.1, bf16[256,128]{1,0:T(8,128)(2,1)} %k2_ref.1, bf16[256,256]{1,0:T(8,128)(2,1)} %v_ref.1, f32[1,128]{1,0:T(1,128)} %bitcast.7, ...), custom_call_target="tpu_custom_call" | custom-call | tf_op jit(solution)/shard_map/pallas_call | solution.py:514
  77.7 0.7 copy.15

commit v7 on v5

--- a/solution.py
+++ b/solution.py
@@ -294,7 +294,6 @@
     for p in range(2):
         up_z(mate, p).start()
     up_far(0)
-    pl.when(inner)(lambda: up_far(1))
     for p in range(pieces):
         dn_y0(p).start()
     for ld in gain_loads + [st_load, ow_load, up_load, dn_load]:
@@ -311,6 +310,8 @@
         for mp in range(2):
             keep = (lane >= mp * qk) & (lane < (mp + 1) * qk)
             qm[mp, i * tok : (i + 1) * tok, :] = jnp.where(keep, qv, 0.0).astype(BF16)
+
+    pl.when(inner)(lambda: up_far(1))
 
     def absorb(block):
         v = block[:, qw:]
@@ -437,7 +438,7 @@
 
     def finish(n):
         arrived(sib_buf.at[n], rsib.at[n])
-        for k in range(ng - 1, 0, -1):
+        for k in range(1, ng):
             g = lax.rem(grp + k, ng)
             rows = pl.ds(pl.multiple_of(g * share, share), share)
             red_snd[n, g] = (part[n, :, rows, :] + sib_buf[n, :, rows, :].astype(F32)).astype(BF16)

time: 78.6 us -> 78.4 us (level)
  no operation moved by 1% of the time
where the time goes in v7:
time: 78.4 us; the launch traced here: 78.3 us
  Pallas kernels  77.6 us (99%)
    pallas_call x1, Pallas kernels, local(): pl.pallas_call(functools.partial(kernel, nsp, ntp, heads, pieces), out_sh...  77.6 us

profile of v7, /device:TPU:0, one launch (start us, length us, event | category | flops | bytes accessed | tf_op | source)
XLA Modules:
  0.0 78.3 jit_solution(12368842826701511469)
XLA Ops:
  0.0 77.6 %shard_map.127 = bf16[64,2048]{1,0:T(8,128)(2,1)S(1)} custom-call(f32[1,2]{1,0:T(1,128)} %bitcast.6, bf16[256,128]{1,0:T(8,128)(2,1)} %q1_ref.1, bf16[256,128]{1,0:T(8,128)(2,1)} %q2_ref.1, bf16[256,128]{1,0:T(8,128)(2,1)} %k1_ref.1, bf16[256,128]{1,0:T(8,128)(2,1)} %k2_ref.1, bf16[256,256]{1,0:T(8,128)(2,1)} %v_ref.1, f32[1,128]{1,0:T(1,128)} %bitcast.7, ...), custom_call_target="tpu_custom_call" | custom-call | tf_op jit(solution)/shard_map/pallas_call | solution.py:515
  77.6 0.7 copy.15
